TPU v7x, 128 devices: a whole 4x4x4 slice. The times are simulated.
128 devices in a mesh: ep: 16 (over z, x), tp: 8 (over y, core).
Axes of the slice: x: 4, y: 4, z: 4, core: 2. Of those that a mesh axis runs over, the one named last changes fastest.
Arguments:
- tokens: bfloat16 [16384, 2048], P(('ep', 'tp')), may hold values from -6 to 6
- routes: int32 [16384, 2], P(('ep', 'tp')), may hold values from 0 to 127, as said below
- gates: float32 [16384, 2], P(('ep', 'tp')), may hold values from 0.1 to 0.6
- w_gate: bfloat16 [128, 2048, 768], P(('ep', 'tp')), may hold values from -0.125 to 0.125
- w_up: bfloat16 [128, 2048, 768], P(('ep', 'tp')), may hold values from -0.125 to 0.125
- w_down: bfloat16 [128, 768, 2048], P(('ep', 'tp')), may hold values from -0.21875 to 0.21875
- moe_out: bfloat16 [16384, 2048], P('ep', 'tp'), may hold values from -16 to 16
- norm_gain: float32 [2048], P('tp'), may hold values from 0.1 to 1.9
- out_grad: bfloat16 [16384, 2048], P('ep', 'tp'), may hold values from -16 to 16
Outputs:
- token_grad: bfloat16 [16384, 2048], P(('ep', 'tp'))
- gates_grad: bfloat16 [16384, 2], P(('ep', 'tp'))
- w_gate_grad: bfloat16 [128, 2048, 768], P(('ep', 'tp'))
- w_up_grad: bfloat16 [128, 2048, 768], P(('ep', 'tp'))
- w_down_grad: bfloat16 [128, 768, 2048], P(('ep', 'tp'))
Inputs may be any that keep to these rules, and one draw needn't show every extreme that they name: `routes`: the two experts of a row differ and lie in one group (expert e is in group e // 32). In the 128 rows of one device the tokens fall into the groups in shares 3/8, 3/8, 1/8, 1/8 of 128, which group takes which share varying. In the rows of one device no expert is named more than 4 times, and one expert is named exactly 4 times in the rows of every device.
All inputs are finite; a program needn't handle non-finite values.
Results may differ from a plain program's by a relative error of at most 0.0071.
Values may be sent and summed in bfloat16 or wider, within the bound.
A program may use at most 128 MiB of HBM per device.

v0:
```python
import math

import jax
import jax.numpy as jnp
from jax import lax
from jax.sharding import PartitionSpec as P

epsilon = 1e-06


def from_everyone(value, axis):
    copies = jnp.broadcast_to(value, (lax.axis_size(axis), *value.shape))
    return lax.all_to_all(copies, axis, split_axis=0, concat_axis=0, tiled=True)


def over_copies(value, axis):
    everything = from_everyone(value, axis)
    return jnp.sum(everything, axis=0)


def packed_total(arrays, axis):
    ravelled, at, outs = (jnp.concatenate([a.reshape(-1) for a in arrays]), 0, [])
    running = over_copies(ravelled, axis)
    for a in arrays:
        outs.append(running[at : at + a.size].reshape(a.shape))
        at += a.size
    return tuple(outs)


def sent_together(arrays, axis, split_dim, concat_dim, along):
    widths = [math.prod(a.shape[along:]) for a in arrays]
    both = jnp.concatenate(
        [a.reshape(*a.shape[:along], w) for a, w in zip(arrays, widths)], axis=along
    )
    result = lax.all_to_all(both, axis, split_axis=split_dim, concat_axis=concat_dim, tiled=True)
    parts = jnp.split(result, [sum(widths[:k]) for k in range(1, len(widths))], axis=along)
    return tuple(
        (b.reshape(*result.shape[:along], *a.shape[along:]) for a, b in zip(arrays, parts))
    )


def contract(left, right, left_dim, right_dim):
    return lax.dot_general(
        left, right, (((left_dim,), (right_dim,)), ((), ())), preferred_element_type=jnp.float32
    )


def slot_ranks(flat_ids, experts):
    one_hot = (flat_ids[:, None] == jnp.arange(experts, dtype=jnp.int32)[None, :]).astype(jnp.int32)
    return jnp.sum((jnp.cumsum(one_hot, axis=0) - one_hot) * one_hot, axis=1)


def local(tokens, routes, gates, w_gate, w_up, w_down, moe_out, norm_gain, out_grad):
    devices = lax.axis_size(("ep", "tp"))
    tok_rows, features = tokens.shape
    top_count = routes.shape[1]
    capacity = 4 * tok_rows // devices
    route_count = tok_rows * top_count
    saved_out = moe_out.astype(jnp.float32)
    scaled = norm_gain[None, :] * out_grad.astype(jnp.float32)
    square_sum, cross_sum = packed_total(
        (jnp.sum(saved_out * saved_out, axis=1), jnp.sum(saved_out * scaled, axis=1)), "tp"
    )
    inv_rms = lax.rsqrt(square_sum / features + epsilon)
    expert_cot = (
        inv_rms[:, None] * scaled - saved_out * (inv_rms**3 * cross_sum / features)[:, None]
    ).astype(jnp.bfloat16)
    flat_ids = routes.reshape(-1)
    own_slots = flat_ids * capacity + slot_ranks(flat_ids, devices)
    route_tokens = jnp.arange(route_count, dtype=jnp.int32) // top_count
    token_of_slot = (
        jnp.full((devices * capacity,), tok_rows, jnp.int32).at[own_slots].set(route_tokens)
    )
    gate_slots = (
        jnp.zeros((devices * capacity,), jnp.bfloat16)
        .at[own_slots]
        .set(gates.reshape(-1).astype(jnp.bfloat16))
        .reshape(devices, capacity)
    )
    token_pad = jnp.concatenate([tokens, jnp.zeros((1, features), jnp.bfloat16)], axis=0)
    token_slots = token_pad[token_of_slot].reshape(devices, capacity, features)
    cot_rows = lax.all_to_all(expert_cot, "tp", split_axis=0, concat_axis=1, tiled=True)
    cot_pad = jnp.concatenate([cot_rows, jnp.zeros((1, features), jnp.bfloat16)], axis=0)
    cot_slots = cot_pad[token_of_slot].reshape(devices, capacity, features)
    token_in, cot_in, gate_in = (
        lax.all_to_all(token_slots, ("ep", "tp"), split_axis=0, concat_axis=0, tiled=True),
        lax.all_to_all(cot_slots, ("ep", "tp"), split_axis=0, concat_axis=0, tiled=True),
        lax.all_to_all(gate_slots, ("ep", "tp"), split_axis=0, concat_axis=0, tiled=True),
    )
    cot_in = cot_in.reshape(devices * capacity, features)
    row_block = token_in.reshape(devices * capacity, features)
    w_gate_one = w_gate[0]
    w_up_one = w_up[0]
    w_down_one = w_down[0]
    pre_gate = jnp.dot(row_block, w_gate_one, preferred_element_type=jnp.float32)
    pre_up = jnp.dot(row_block, w_up_one, preferred_element_type=jnp.float32)
    sigmoid_gate = jax.nn.sigmoid(pre_gate)
    activated = pre_gate * sigmoid_gate
    hidden = activated * pre_up
    hid_grad = contract(cot_in, w_down_one, 1, 1)
    gate_grad = jnp.sum(hidden * hid_grad, axis=1).astype(jnp.bfloat16)
    weight = gate_in.reshape(-1).astype(jnp.float32)[:, None]
    d_hidden = weight * hid_grad
    d_gate = (d_hidden * pre_up * sigmoid_gate * (1.0 + pre_gate * (1.0 - sigmoid_gate))).astype(
        jnp.bfloat16
    )
    d_up = (d_hidden * activated).astype(jnp.bfloat16)
    token_back = (contract(d_gate, w_gate_one, 1, 1) + contract(d_up, w_up_one, 1, 1)).astype(
        jnp.bfloat16
    )
    scaled_cot = (weight * cot_in.astype(jnp.float32)).astype(jnp.bfloat16)
    grad_gate = contract(row_block, d_gate, 0, 0).astype(jnp.bfloat16)
    grad_up = contract(row_block, d_up, 0, 0).astype(jnp.bfloat16)
    grad_down = contract(hidden.astype(jnp.bfloat16), scaled_cot, 0, 0).astype(jnp.bfloat16)
    back_rows, back_gates = sent_together(
        (token_back.reshape(devices, capacity, features), gate_grad.reshape(devices, capacity)),
        ("ep", "tp"),
        0,
        0,
        2,
    )
    per_route = back_rows.reshape(devices * capacity, features)[own_slots]
    token_grad = jnp.sum(
        per_route.astype(jnp.float32).reshape(tok_rows, top_count, features), axis=1
    ).astype(jnp.bfloat16)
    gates_grad = back_gates.reshape(-1)[own_slots].reshape(tok_rows, top_count)
    return (token_grad, gates_grad, grad_gate[None], grad_up[None], grad_down[None])


def solution(mesh):
    in_specs = (
        P(("ep", "tp"), None),
        P(("ep", "tp"), None),
        P(("ep", "tp"), None),
        P(("ep", "tp"), None, None),
        P(("ep", "tp"), None, None),
        P(("ep", "tp"), None, None),
        P("ep", "tp"),
        P("tp"),
        P("ep", "tp"),
    )
    out_specs = (
        P(("ep", "tp"), None),
        P(("ep", "tp"), None),
        P(("ep", "tp"), None, None),
        P(("ep", "tp"), None, None),
        P(("ep", "tp"), None, None),
    )
    return jax.shard_map(local, mesh=mesh, in_specs=in_specs, out_specs=out_specs, check_vma=False)
```

profile of v0, /device:TPU:1, one launch (start us, length us, event | category | flops | bytes accessed | tf_op | source)
XLA Modules:
  0.0 207.3 jit_solution(3335858784704392693)
XLA Ops:
  3.1 6.0 %all-to-all-start.1 = ((f32[8,1,2048]{2,1,0:T(1,128)}), f32[8,1,2048]{2,1,0:T(1,128)S(1)}, u32[]{:S(2)}, u32[]{:S(2)}) async-start(f32[8,1,2048]{2,1,0:T(1,128)} %broadcast_in_dim.15), calls=%async_computation.1 | async-start | bytes 131072 | tf_op jit(solution)/shard_map/all_to_all | solution.py:13
  14.9 10.3 %all-to-all-start = ((bf16[128,1,4]{2,1,0:T(2,128)(2,1)}), bf16[128,1,4]{2,1,0:T(2,128)(2,1)S(1)}, u32[]{:S(2)}, u32[]{:S(2)}) async-start(bf16[128,1,4]{2,1,0:T(2,128)(2,1)} %all_to_all.43), calls=%async_computation | async-start | bytes 131072 | tf_op jit(solution)/shard_map/all_to_all | solution.py:88
  27.6 7.1 %all-to-all-done = bf16[128,1,4]{2,1,0:T(2,128)(2,1)S(1)} async-done(((bf16[128,1,4]{2,1,0:T(2,128)(2,1)}), bf16[128,1,4]{2,1,0:T(2,128)(2,1)S(1)}, u32[]{:S(2)}, u32[]{:S(2)}) %all-to-all-start) | async-done | bytes 1056 | tf_op jit(solution)/shard_map/all_to_all | solution.py:88
  34.8 4.8 %all-to-all-start.2 = ((bf16[8,128,256]{2,1,0:T(8,128)(2,1)}), bf16[8,128,256]{2,1,0:T(8,128)(2,1)}, u32[]{:S(2)}, u32[]{:S(2)}) async-start(bf16[8,128,256]{2,1,0:T(8,128)(2,1)} %bitcast.52), calls=%async_computation.2 | async-start | bytes 1048576 | tf_op jit(solution)/shard_map/all_to_all | solution.py:82
  42.9 6.4 %gather_fusion.1 = bf16[512,2048]{1,0:T(8,128)(2,1)} fusion(bf16[129,2048]{1,0:T(8,128)(2,1)} %concatenate.14, s32[1024]{0:T(1024)S(1)} %pad_clamp_fusion.1), kind=kCustom, calls=%fused_computation.1 | custom fusion | bytes 4196352 | tf_op jit(solution)/shard_map/gather | solution.py:81
  49.3 4.1 %reshape.118 = bf16[128,4,2048]{2,1,0:T(4,128)(2,1)} reshape(bf16[512,2048]{1,0:T(8,128)(2,1)} %gather_fusion.1) | data formatting | bytes 4194304 | tf_op jit(solution)/shard_map/reshape | solution.py:81
  53.4 5.9 %all-to-all-start.4 = ((bf16[128,4,2048]{2,1,0:T(4,128)(2,1)}), bf16[128,4,2048]{2,1,0:T(4,128)(2,1)}, u32[]{:S(2)}, u32[]{:S(2)}) async-start(bf16[128,4,2048]{2,1,0:T(4,128)(2,1)} %reshape.118), calls=%async_computation.4 | async-start | bytes 4194304 | tf_op jit(solution)/shard_map/all_to_all | solution.py:86
  61.2 6.3 %gather_fusion = bf16[512,2048]{1,0:T(8,128)(2,1)} fusion(bf16[129,2048]{1,0:T(8,128)(2,1)} %concatenate.13, s32[1024]{0:T(1024)S(1)} %pad_clamp_fusion.1), kind=kCustom, calls=%fused_computation | custom fusion | bytes 4196352 | tf_op jit(solution)/shard_map/gather | solution.py:84
  67.6 4.1 %reshape.116 = bf16[128,4,2048]{2,1,0:T(4,128)(2,1)} reshape(bf16[512,2048]{1,0:T(8,128)(2,1)} %gather_fusion) | data formatting | bytes 4194304 | tf_op jit(solution)/shard_map/reshape | solution.py:84
  71.7 17.3 %all-to-all-done.4 = bf16[128,4,2048]{2,1,0:T(4,128)(2,1)} async-done(((bf16[128,4,2048]{2,1,0:T(4,128)(2,1)}), bf16[128,4,2048]{2,1,0:T(4,128)(2,1)}, u32[]{:S(2)}, u32[]{:S(2)}) %all-to-all-start.4) | async-done | bytes 2097184 | tf_op jit(solution)/shard_map/all_to_all | solution.py:86
  89.0 5.8 %all-to-all-start.3 = ((bf16[128,4,2048]{2,1,0:T(4,128)(2,1)}), bf16[128,4,2048]{2,1,0:T(4,128)(2,1)}, u32[]{:S(2)}, u32[]{:S(2)}) async-start(bf16[128,4,2048]{2,1,0:T(4,128)(2,1)} %reshape.116), calls=%async_computation.3 | async-start | bytes 4194304 | tf_op jit(solution)/shard_map/all_to_all | solution.py:87
  95.1 3.9 %reshape.119 = bf16[512,2048]{1,0:T(8,128)(2,1)} reshape(bf16[128,4,2048]{2,1,0:T(4,128)(2,1)} %all-to-all-done.4) | data formatting | bytes 4194304 | tf_op jit(solution)/shard_map/reshape | solution.py:91
  99.1 5.5 %fusion.6 = f32[512,768]{1,0:T(8,128)} fusion(bf16[512,2048]{1,0:T(8,128)(2,1)} %reshape.119, bf16[1,2048,768]{2,1,0:T(8,128)(2,1)} %param.13), kind=kOutput, calls=%fused_computation.17 | convolution fusion | flops 1610612736 | bytes 6815744 | tf_op jit(solution)/shard_map/dot_general | solution.py:96
  104.6 20.1 %all-to-all-done.3 = bf16[128,4,2048]{2,1,0:T(4,128)(2,1)} async-done(((bf16[128,4,2048]{2,1,0:T(4,128)(2,1)}), bf16[128,4,2048]{2,1,0:T(4,128)(2,1)}, u32[]{:S(2)}, u32[]{:S(2)}) %all-to-all-start.3) | async-done | bytes 2097184 | tf_op jit(solution)/shard_map/all_to_all | solution.py:87
  124.7 3.9 %reshape.117 = bf16[512,2048]{1,0:T(8,128)(2,1)} reshape(bf16[128,4,2048]{2,1,0:T(4,128)(2,1)} %all-to-all-done.3) | data formatting | bytes 4194304 | tf_op jit(solution)/shard_map/reshape | solution.py:90
  128.7 4.5 %fusion.8 = f32[512,768]{1,0:T(8,128)S(1)} fusion(bf16[512,2048]{1,0:T(8,128)(2,1)} %reshape.117, bf16[1,768,2048]{2,1,0:T(8,128)(2,1)} %param.14), kind=kOutput, calls=%fused_computation.19 | convolution fusion | flops 1610612736 | bytes 6815744 | tf_op jit(solution)/shard_map/dot_general | solution.py:43
  133.2 3.7 %multiply_convert_fusion.3 = (bf16[512,768]{1,0:T(8,128)(2,1)S(1)}, bf16[512]{0:T(512)(128)(2,1)S(1)}, bf16[512,768]{1,0:T(8,128)(2,1)S(1)}, f32[512,768]{1,0:T(8,128)}) fusion(f32[512,768]{1,0:T(8,128)S(1)} %copy-done.12, f32[512,768]{1,0:T(8,128)S(1)} %fusion.8, f32[512]{0:T(512)S(1)} %reshape.123, bf16[512,2048]{1,0:T(8,128)(2,1)S(1)} %copy-done.3, ...), kind=kOutput, calls=%fused_computation.28 | convolution fusion | flops 1617296896 | bytes 11537408 | tf_op jit(solution)/shard_map/dot_general | solution.py:95
  148.1 4.7 %all-to-all-start.5 = ((bf16[128,4,2049]{2,1,0:T(4,128)(2,1)}), bf16[128,4,2049]{2,1,0:T(4,128)(2,1)S(1)}, u32[]{:S(2)}, u32[]{:S(2)}) async-start(bf16[128,4,2049]{2,1,0:T(4,128)(2,1)} %pad_maximum_fusion), calls=%async_computation.5 | async-start | bytes 4456448 | tf_op jit(solution)/shard_map/all_to_all | solution.py:35
  152.9 5.4 %fusion.10 = bf16[1,2048,768]{2,1,0:T(8,128)(2,1)} fusion(bf16[512,2048]{1,0:T(8,128)(2,1)} %reshape.119, bf16[512,768]{1,0:T(8,128)(2,1)} %copy-done.11), kind=kOutput, calls=%fused_computation.21 | convolution fusion | flops 1612185600 | bytes 6029312 | tf_op jit(solution)/shard_map/dot_general | solution.py:43
  161.9 3.7 %fusion.12 = bf16[1,768,2048]{2,1,0:T(8,128)(2,1)} fusion(bf16[512,2048]{1,0:T(8,128)(2,1)S(1)} %copy-done.5, f32[512]{0:T(512)S(1)} %reshape.123, f32[512,768]{1,0:T(8,128)S(1)} %copy-done.13, f32[512,768]{1,0:T(8,128)S(1)} %copy-done.14), kind=kOutput, calls=%fused_computation.23 | convolution fusion | flops 1617690624 | bytes 8390656 | tf_op jit(solution)/shard_map/dot_general | solution.py:43
  165.6 18.9 %all-to-all-done.5 = bf16[128,4,2049]{2,1,0:T(4,128)(2,1)S(1)} async-done(((bf16[128,4,2049]{2,1,0:T(4,128)(2,1)}), bf16[128,4,2049]{2,1,0:T(4,128)(2,1)S(1)}, u32[]{:S(2)}, u32[]{:S(2)}) %all-to-all-start.5) | async-done | bytes 2098208 | tf_op jit(solution)/shard_map/all_to_all | solution.py:35
  187.0 3.9 %reshape.121 = bf16[512,2048]{1,0:T(8,128)(2,1)} reshape(bf16[128,4,2048]{2,1,0:T(4,128)(2,1)} %split.8) | data formatting | bytes 4194304 | tf_op jit(solution)/shard_map/reshape | solution.py:122
  190.9 5.3 %gather_fusion.2 = bf16[256,2048]{1,0:T(8,128)(2,1)} fusion(bf16[512,2048]{1,0:T(8,128)(2,1)} %reshape.121, s32[1024]{0:T(1024)S(1)} %pad_clamp_fusion), kind=kCustom, calls=%fused_computation.2 | custom fusion | bytes 2098176 | tf_op jit(solution)/shard_map/gather | solution.py:122
  198.8 4.6 %reduce_sum.65 = bf16[128,2048]{1,0:T(8,128)(2,1)} reduce(bf16[128,2,2048]{2,1,0:T(2,128)(2,1)} %gather.17, bf16[]{:T(256)} %constant.17.clone.1), dimensions={1}, to_apply=%region_9.10 | reduce | flops 262144 | bytes 1572866 | tf_op jit(solution)/shard_map/reduce_sum | solution.py:123
  (82 shorter events, 39.8 us)
Async XLA Ops:
  0.6 132.5 %copy-start = (bf16[1,2048,768]{2,1,0:T(8,128)(2,1)S(1)}, bf16[1,2048,768]{2,1,0:T(8,128)(2,1)}, u32[]{:S(2)}) copy-start(bf16[1,2048,768]{2,1,0:T(8,128)(2,1)} %param.12) | copy-start | bytes 9437188
  0.6 24.7 %copy-start.6 = (f32[256]{0:T(256)S(1)}, f32[256]{0:T(256)}, u32[]{:S(2)}) copy-start(f32[256]{0:T(256)} %param.16) | copy-start | bytes 3076
  0.7 11.0 %copy-start.8 = (f32[128,2]{0,1:T(2,128)S(1)}, f32[128,2]{0,1:T(2,128)}, u32[]{:S(2)}) copy-start(f32[128,2]{0,1:T(2,128)} %param.11) | copy-start | bytes 3076
  3.1 11.8 %all-to-all-start.1 = ((f32[8,1,2048]{2,1,0:T(1,128)}), f32[8,1,2048]{2,1,0:T(1,128)S(1)}, u32[]{:S(2)}, u32[]{:S(2)}) async-start(f32[8,1,2048]{2,1,0:T(1,128)} %broadcast_in_dim.15), calls=%async_computation.1 | async-start | bytes 131072 | tf_op jit(solution)/shard_map/all_to_all | solution.py:13
  14.9 19.9 %all-to-all-start = ((bf16[128,1,4]{2,1,0:T(2,128)(2,1)}), bf16[128,1,4]{2,1,0:T(2,128)(2,1)S(1)}, u32[]{:S(2)}, u32[]{:S(2)}) async-start(bf16[128,1,4]{2,1,0:T(2,128)(2,1)} %all_to_all.43), calls=%async_computation | async-start | bytes 131072 | tf_op jit(solution)/shard_map/all_to_all | solution.py:88
  34.8 18.6 %all-to-all-start.2 = ((bf16[8,128,256]{2,1,0:T(8,128)(2,1)}), bf16[8,128,256]{2,1,0:T(8,128)(2,1)}, u32[]{:S(2)}, u32[]{:S(2)}) async-start(bf16[8,128,256]{2,1,0:T(8,128)(2,1)} %bitcast.52), calls=%async_computation.2 | async-start | bytes 1048576 | tf_op jit(solution)/shard_map/all_to_all | solution.py:82
  53.4 35.7 %all-to-all-start.4 = ((bf16[128,4,2048]{2,1,0:T(4,128)(2,1)}), bf16[128,4,2048]{2,1,0:T(4,128)(2,1)}, u32[]{:S(2)}, u32[]{:S(2)}) async-start(bf16[128,4,2048]{2,1,0:T(4,128)(2,1)} %reshape.118), calls=%async_computation.4 | async-start | bytes 4194304 | tf_op jit(solution)/shard_map/all_to_all | solution.py:86
  89.0 35.7 %all-to-all-start.3 = ((bf16[128,4,2048]{2,1,0:T(4,128)(2,1)}), bf16[128,4,2048]{2,1,0:T(4,128)(2,1)}, u32[]{:S(2)}, u32[]{:S(2)}) async-start(bf16[128,4,2048]{2,1,0:T(4,128)(2,1)} %reshape.116), calls=%async_computation.3 | async-start | bytes 4194304 | tf_op jit(solution)/shard_map/all_to_all | solution.py:87
  128.7 4.5 %copy-start.3 = (bf16[512,2048]{1,0:T(8,128)(2,1)S(1)}, bf16[512,2048]{1,0:T(8,128)(2,1)}, u32[]{:S(2)}) copy-start(bf16[512,2048]{1,0:T(8,128)(2,1)} %reshape.119) | copy-start | bytes 6291460
  128.7 4.5 %copy-start.12 = (f32[512,768]{1,0:T(8,128)S(1)}, f32[512,768]{1,0:T(8,128)}, u32[]{:S(2)}) copy-start(f32[512,768]{1,0:T(8,128)} %fusion.6) | copy-start | bytes 4718596
  136.9 1.8 copy-start.11
  136.9 1.8 copy-start.9
  136.9 2.5 %copy-start.7 = (bf16[1,2048,768]{2,1,0:T(8,128)(2,1)S(1)}, bf16[1,2048,768]{2,1,0:T(8,128)(2,1)}, u32[]{:S(2)}) copy-start(bf16[1,2048,768]{2,1,0:T(8,128)(2,1)} %param.13) | copy-start | bytes 9437188
  148.1 36.4 %all-to-all-start.5 = ((bf16[128,4,2049]{2,1,0:T(4,128)(2,1)}), bf16[128,4,2049]{2,1,0:T(4,128)(2,1)S(1)}, u32[]{:S(2)}, u32[]{:S(2)}) async-start(bf16[128,4,2049]{2,1,0:T(4,128)(2,1)} %pad_maximum_fusion), calls=%async_computation.5 | async-start | bytes 4456448 | tf_op jit(solution)/shard_map/all_to_all | solution.py:35
  152.8 5.4 %copy-start.4 = (bf16[512,2048]{1,0:T(8,128)(2,1)S(1)}, bf16[512,2048]{1,0:T(8,128)(2,1)}, u32[]{:S(2)}) copy-start(bf16[512,2048]{1,0:T(8,128)(2,1)} %reshape.119) | copy-start | bytes 6291460
  152.8 5.4 %copy-start.10 = (bf16[512,768]{1,0:T(8,128)(2,1)S(1)}, bf16[512,768]{1,0:T(8,128)(2,1)}, u32[]{:S(2)}) copy-start(bf16[512,768]{1,0:T(8,128)(2,1)} %copy-done.9) | copy-start | bytes 2359300
  158.3 3.6 %copy-start.5 = (bf16[512,2048]{1,0:T(8,128)(2,1)S(1)}, bf16[512,2048]{1,0:T(8,128)(2,1)}, u32[]{:S(2)}) copy-start(bf16[512,2048]{1,0:T(8,128)(2,1)} %reshape.117) | copy-start | bytes 6291460
  158.3 3.6 %copy-start.13 = (f32[512,768]{1,0:T(8,128)S(1)}, f32[512,768]{1,0:T(8,128)}, u32[]{:S(2)}) copy-start(f32[512,768]{1,0:T(8,128)} %fusion.6) | copy-start | bytes 4718596
  158.3 3.6 %copy-start.14 = (f32[512,768]{1,0:T(8,128)S(1)}, f32[512,768]{1,0:T(8,128)}, u32[]{:S(2)}) copy-start(f32[512,768]{1,0:T(8,128)} %get-tuple-element.32) | copy-start | bytes 4718596
  184.5 2.5 %copy-start.2 = (bf16[128,4,2049]{2,1,0:T(4,128)(2,1)}, bf16[128,4,2049]{2,1,0:T(4,128)(2,1)S(1)}, u32[]{:S(2)}) copy-start(bf16[128,4,2049]{2,1,0:T(4,128)(2,1)S(1)} %all-to-all-done.5) | copy-start | bytes 6294532
  190.9 16.4 %copy-start.1 = (bf16[1,2048,768]{2,1,0:T(8,128)(2,1)S(1)}, bf16[1,2048,768]{2,1,0:T(8,128)(2,1)}, u32[]{:S(2)}) copy-start(bf16[1,2048,768]{2,1,0:T(8,128)(2,1)} %param.12) | copy-start | bytes 9437188
where the time goes:
time: 209 us; the launch traced here: 207 us
  waiting for transfers between devices  63.6 us (30%)
  local copies, waits for them, and re-layouts  61.4 us (29%)
  starting transfers between devices  37.5 us (18%)
  matrix products  31.3 us (15%)
  other arithmetic  12.6 us (6%)
    dot_general x6, matrix products, contract(): lax.dot_general(left, right, (((left_dim,), (right_dim,)), ((), ())), pre...  22.1 us
    all_to_all x1, waiting for transfers between devices, local(): lax.all_to_all(cot_slots, ('ep', 'tp'), split_axis=0, concat_axis=0, tile...  20.1 us
    all_to_all x1, waiting for transfers between devices, sent_together(): lax.all_to_all(both, axis, split_axis=split_dim, concat_axis=concat_dim,...  18.9 us
    all_to_all x1, waiting for transfers between devices, local(): lax.all_to_all(token_slots, ('ep', 'tp'), split_axis=0, concat_axis=0, ti...  17.3 us
    all_to_all x1, starting transfers between devices, local(): lax.all_to_all(gate_slots, ('ep', 'tp'), split_axis=0, concat_axis=0, til...  10.3 us
    gather x2, local copies, waits for them, and re-layouts, local(): per_route = back_rows.reshape(devices * capacity, features)[own_slots]  7.88 us
    all_to_all x1, waiting for transfers between devices, local(): lax.all_to_all(gate_slots, ('ep', 'tp'), split_axis=0, concat_axis=0, til...  7.14 us
    gather x1, local copies, waits for them, and re-layouts, local(): token_slots = token_pad[token_of_slot].reshape(devices, capacity, features)  6.35 us
  transfers between devices with their start and end apart: 6, of which 4 were waited for; matrix products, arithmetic and copies ran while one was open for 27% of the time, Pallas kernels for 0%

commit v1 on v0

v1 whole, which is shorter than its diff:
```python
import jax
import jax.numpy as jnp
from jax import lax
from jax.experimental import pallas as pl
from jax.experimental.pallas import tpu as pltpu
from jax.sharding import PartitionSpec as P

F32 = jnp.float32
BF16 = jnp.bfloat16
MESH = pl.DeviceIdType.MESH
VMEM = pl.BlockSpec(memory_space=pltpu.VMEM)
SMEM = pl.BlockSpec(memory_space=pltpu.SMEM)
ANY = pl.BlockSpec(memory_space=pl.ANY)
SIZE = {"z": 4, "x": 4, "t": 8}
AXIS = {"z": 0, "x": 1, "t": 2}
epsilon = 1e-06

PLAN = (
    "bar", "T1t", "T0x", "stat", "T7x", "T4z", "T5z", "T2t", "cot", "T3x", "T1z", "T4x",
    "T7z", "T0z", "T2x", "T6t", "T1x", "T5t", "T3z", "table", "C0t", "C1x", "T4t", "C3t",
    "T2z", "C2x", "C4z", "C7x", "T3t", "C1z", "C0x", "C6t", "C2z", "T0t", "T5x", "C3z",
    "C5x", "C1t", "T6z", "C0z", "C6x", "C2t", "A1", "C3x", "C4x", "A2", "T6x", "C7z",
    "C5t", "T7t", "A0", "C6z", "B0", "D0", "R1z", "C7t", "B1", "C5z", "R2x", "R0x",
    "C4t", "D1", "R3z", "A3", "R1t", "B3", "R6z", "R2t", "B2", "R4z", "R0t", "R1x",
    "D2", "R3x", "R5z", "D3", "R7t", "R6x", "R2z", "R4t", "R5x", "R7z", "R3t", "R0z",
    "R6t", "R4x", "R7x", "R5t",
)


def iota(shape, dim):
    return lax.broadcasted_iota(jnp.int32, shape, dim)


def dot(a, b, a_dim=1, b_dim=0):
    return lax.dot_general(
        a, b, (((a_dim,), (b_dim,)), ((), ())), preferred_element_type=F32
    )


def to_rows():
    i, j = iota((256, 256), 0), iota((256, 256), 1)
    return (((i >> 5) == (j & 7)) & ((i & 31) == (j >> 3))).astype(F32).astype(BF16)


def to_tiles():
    i, j = iota((256, 256), 0), iota((256, 256), 1)
    return (((i >> 3) == (j & 31)) & ((i & 7) == (j >> 5))).astype(F32).astype(BF16)


def tile_pair(perm, pieces, put):
    for pair in range(2):
        both = jnp.concatenate(
            [jnp.concatenate(pieces(2 * pair + j), axis=0) for j in range(2)], axis=1
        )
        out = dot(perm, both).astype(BF16)
        for j in range(2):
            put(2 * pair + j, out[:, 128 * j : 128 * (j + 1)])


def row_pair(perm, tiles, put):
    for pair in range(2):
        both = jnp.concatenate([tiles(2 * pair + j) for j in range(2)], axis=1)
        out = dot(perm, both).astype(BF16)
        for j in range(2):
            for b in range(8):
                put(2 * pair + j, b, out[32 * b : 32 * (b + 1), 128 * j : 128 * (j + 1)])


def route_kernel(
    routes_ref, gates_ref, tokens_ref, moe_ref, grad_ref, gain_ref,
    index_ref, spot_ref, gate_ref, pick_ref, table_ref, stat_ref,
):
    head = jnp.concatenate(
        [routes_ref[...].astype(F32), gates_ref[...], jnp.zeros((4, 128), F32)], axis=0
    )
    cols = head.T
    lane, row = iota((128, 128), 1), iota((128, 128), 0)
    lane_f = lane.astype(F32)
    below = (lane < row).astype(F32).astype(BF16)
    hot = [(cols[:, k : k + 1] == lane_f).astype(F32) for k in range(2)]
    seen = dot(below, (hot[0] + hot[1]).astype(BF16))
    rank = [jnp.sum(hot[k] * seen, axis=1, keepdims=True) for k in range(2)]
    number = (row + 1).astype(F32)
    index = jnp.zeros((128, 128), F32)
    gate = jnp.zeros((128, 128), F32)
    for k in range(2):
        at = lane_f == rank[k]
        one = hot[k].astype(BF16)
        index += dot(jnp.where(at, number, 0.0).astype(BF16), one, 0, 0)
        gate += dot(one, jnp.where(at, cols[:, 2 + k : 3 + k], 0.0).astype(BF16), 0, 0)
    index_ref[...] = index[:8].astype(jnp.int32)
    gate_ref[:, 0, :] = gate
    pick = jnp.zeros((128, 128), F32)
    for k in range(2):
        pick = jnp.where(lane == k, rank[k] * 256.0 + cols[:, k : k + 1], pick)
        pick = jnp.where(lane == 2 + k, cols[:, k : k + 1], pick)
        pick = jnp.where(lane == 4 + k, rank[k], pick)
    pick_ref[...] = pick
    spot_ref[...] = pick.T[:8].astype(jnp.int32)
    perm = to_tiles()
    for h in range(2):
        table_ref[h, 0] = jnp.zeros((8, 128), BF16)

        def pieces(g, h=h):
            return [
                tokens_ref[32 * g : 32 * (g + 1), 1024 * h + 128 * b : 1024 * h + 128 * (b + 1)]
                for b in range(8)
            ]

        def put(g, tiles, h=h):
            table_ref[h, 1 + 32 * g : 33 + 32 * g] = tiles.reshape(32, 8, 128)

        tile_pair(perm, pieces, put)
    for b in range(8):
        saved = moe_ref[128 * b : 128 * (b + 1), :].astype(F32)
        scaled = gain_ref[...] * grad_ref[128 * b : 128 * (b + 1), :].astype(F32)
        for s, prod in enumerate((saved * saved, saved * scaled)):
            part = (prod[:, :128] + prod[:, 128:]).T
            stat_ref[s, b : b + 1, :] = jnp.sum(part, axis=0, keepdims=True)


def coords():
    ep = lax.axis_index("ep")
    return {"z": ep // 4, "x": ep % 4, "t": lax.axis_index("tp")}


def peers(dim, here):
    if dim != "t":
        return [(here + k) % 4 for k in (1, 3, 2)]
    return [
        (here // 2 + dy) % 4 * 2 + (here % 2 + dc) % 2
        for dy, dc in ((1, 0), (3, 0), (1, 1), (3, 1), (2, 0), (2, 1), (0, 1))
    ]


def others():
    me = coords()
    for dim in "zxt":
        for p in peers(dim, me[dim]):
            place = {**me, dim: p}
            yield dim, p, (place["z"] * 4 + place["x"], place["t"])


def greet():
    for _, _, device in others():
        pl.semaphore_signal(
            pltpu.get_barrier_semaphore(), inc=1, device_id=device, device_id_type=MESH
        )


def cut(ref, axis, index):
    return ref.at[(slice(None),) * axis + (index,)]


class Hop:
    def __init__(self, dim, axis, src, dst, sems, whole=False):
        self.dim, self.axis, self.whole = dim, axis, whole
        self.src, self.dst, (self.ssem, self.rsem, self.lsem) = src, dst, sems

    def piece(self, index):
        return self.src if self.whole else cut(self.src, self.axis, index)

    def start(self):
        mine = coords()[self.dim]
        for dim, p, device in others():
            if dim == self.dim:
                pltpu.make_async_remote_copy(
                    self.piece(p),
                    cut(self.dst, self.axis, mine),
                    self.ssem,
                    self.rsem,
                    device_id=device,
                    device_id_type=MESH,
                ).start()
        pltpu.make_async_copy(self.piece(mine), cut(self.dst, self.axis, mine), self.lsem).start()

    def remote_part(self):
        return cut(self.dst, self.axis, slice(0, SIZE[self.dim] - 1))

    def arrived(self):
        part = self.remote_part()
        pltpu.make_async_copy(part, part, self.rsem).wait()
        one = cut(self.dst, self.axis, 0)
        pltpu.make_async_copy(one, one, self.lsem).wait()

    def left(self):
        part = self.remote_part()
        pltpu.make_async_copy(part, part, self.ssem).wait()


def pack(index_ref, rank, table_ref, half, dst):
    def body(i, carry):
        for t in range(8):
            dst[i // 4, i % 4, t] = table_ref[half, index_ref[rank, i * 8 + t]]
        return carry

    lax.fori_loop(0, 16, body, 0)


def mega_kernel(
    index_ref, gate_ref, table_ref, stat_ref, moe_ref, grad_ref, gain_ref, wg_any, wu_any, wd_any,
    back_ref, slope_ref, x_rows, d_gate, d_up, hidden, scaled_cot,
    wg, wu, wd, t_src, t_one, t_two, t_out, c_src, c_one, c_two, c_out, r_src, r_one, r_two,
    g_one, g_two, g_out, q_src, q_one, q_two, s_in, cot_out, cot_in, cot_table,
    pre_gate, pre_up, cot_rows, back_rows, slope,
    ssem, rsem, lsem, misc, wsem,
):
    greet()
    weights = [
        pltpu.make_async_copy(a, b, wsem.at[i])
        for i, (a, b) in enumerate(((wg_any, wg), (wu_any, wu), (wd_any, wd)))
    ]
    for w in weights:
        w.start()
    slope[...] = jnp.zeros((128, 128), F32)
    unpack_perm, pack_perm = to_rows(), to_tiles()
    families = {
        "T": (t_src, t_one, t_two, t_out),
        "C": (c_src, c_one, c_two, c_out),
        "R": (r_src, r_one, r_two, back_ref),
    }
    hops = {}
    every = []

    def small(i):
        return tuple(misc.at[i, j] for j in range(3))

    stat_hop = Hop("t", 0, stat_ref, s_in, small(0), whole=True)
    cot_hop = Hop("t", 0, cot_out, cot_in, small(1))
    gate_hops = [
        Hop(d, AXIS[d], a, b, small(2 + i))
        for i, (d, a, b) in enumerate(
            (("x", gate_ref, g_one), ("t", g_one, g_two), ("z", g_two, g_out))
        )
    ]
    slope_hops = [
        Hop(d, AXIS[d], a, b, small(5 + i))
        for i, (d, a, b) in enumerate(
            (("x", q_src, q_one), ("t", q_one, q_two), ("z", q_two, slope_ref))
        )
    ]

    def begin(hop):
        hop.start()
        every.append(hop)

    def norm_statistics():
        begin(stat_hop)
        begin(gate_hops[0])

    def cotangents():
        stat_hop.arrived()
        total = s_in[0]
        for p in range(1, 8):
            total += s_in[p]
        inv = lax.rsqrt(total[0] / 2048.0 + epsilon)
        cols = jnp.concatenate([inv, inv**3 * total[1] / 2048.0], axis=0).T

        for b in range(8):
            rows = slice(128 * b, 128 * (b + 1))
            scaled = gain_ref[...] * grad_ref[rows, :].astype(F32)
            saved = moe_ref[rows, :].astype(F32)
            cot_out[b] = (
                cols[:, b : b + 1] * scaled - saved * cols[:, 8 + b : 9 + b]
            ).astype(BF16)
        begin(cot_hop)
        gate_hops[0].arrived()
        begin(gate_hops[1])

    def cotangent_table():
        cot_hop.arrived()
        for h in range(2):
            cot_table[h, 0] = jnp.zeros((8, 128), BF16)

            def pieces(g, h=h):
                return [
                    cot_in[4 * h + b // 2, 32 * g : 32 * (g + 1), b % 2 * 128 : b % 2 * 128 + 128]
                    for b in range(8)
                ]

            def put(g, tiles, h=h):
                cot_table[h, 1 + 32 * g : 33 + 32 * g] = tiles.reshape(32, 8, 128)

            tile_pair(pack_perm, pieces, put)
        gate_hops[1].arrived()
        begin(gate_hops[2])

    def unpack(src, dst, row, half):
        def put(g, b, rows):
            dst[
                row + 32 * g : row + 32 * (g + 1), 1024 * half + 128 * b : 1024 * half + 128 * b + 128
            ] = rows

        row_pair(unpack_perm, lambda g: src[g].reshape(256, 128), put)

    def hidden_inputs(r):
        if r == 1:
            weights[0].wait()
            weights[1].wait()
        for h in range(2):
            hops["T", 2 * r + h][2].arrived()
            unpack(t_out.at[2 * r + h], x_rows, 128 * r, h)

        def body(n, carry):
            cols = pl.ds(pl.multiple_of(n * 256, 256), 256)
            x = x_rows[128 * r : 128 * (r + 1), :]
            pre_gate[r, :, cols] = dot(x, wg[:, cols])
            pre_up[r, :, cols] = dot(x, wu[:, cols])
            return carry

        lax.fori_loop(0, 3, body, 0)

    def half_back(r, h):
        rows = slice(128 * r, 128 * (r + 1))

        def body(n, carry):
            wide = pl.ds(pl.multiple_of(1024 * h + n * 256, 256), 256)
            total = dot(d_gate[rows, :], wg[wide, :], 1, 1) + dot(d_up[rows, :], wu[wide, :], 1, 1)
            back_rows[:, pl.ds(pl.multiple_of(n * 256, 256), 256)] = total.astype(BF16)
            return carry

        lax.fori_loop(0, 4, body, 0)

        def pieces(g):
            return [
                back_rows[32 * g : 32 * (g + 1), 128 * b : 128 * (b + 1)] for b in range(8)
            ]

        def put(g, tiles):
            r_src[2 * r + h, g] = tiles.reshape(4, 8, 8, 128)

        tile_pair(pack_perm, pieces, put)

    def slopes(r):
        if r == 0:
            weights[2].wait()
            gate_hops[2].arrived()
        for h in range(2):
            hops["C", 2 * r + h][2].arrived()
            unpack(c_out.at[2 * r + h], cot_rows, 0, h)
        gates = jnp.concatenate(
            [g_out[z, x][:, 0, :] for z in range(4) for x in range(4)], axis=0
        )
        gate = gates[:, r : r + 1]
        rows = slice(128 * r, 128 * (r + 1))

        def body(n, carry):
            cols = pl.ds(pl.multiple_of(n * 256, 256), 256)
            hid_grad = dot(cot_rows[...], wd[cols, :], 1, 1)
            p_gate, p_up = pre_gate[r, :, cols], pre_up[r, :, cols]
            sig = jax.nn.sigmoid(p_gate)
            act = p_gate * sig
            hid = act * p_up
            d_hid = gate * hid_grad
            d_gate[rows, cols] = (d_hid * p_up * sig * (1.0 + p_gate * (1.0 - sig))).astype(BF16)
            d_up[rows, cols] = (d_hid * act).astype(BF16)
            hidden[rows, cols] = hid.astype(BF16)
            return carry + jnp.sum(hid * hid_grad, axis=1, keepdims=True)

        total = lax.fori_loop(0, 3, body, jnp.zeros((128, 1), F32))
        slope[...] = jnp.where(iota((128, 128), 1) == r, total, slope[...])
        scaled_cot[rows, :] = (gate * cot_rows[...].astype(F32)).astype(BF16)
        half_back(r, 0)

    def rest(r):
        half_back(r, 1)
        if r == 3:
            for z in range(4):
                for x in range(4):
                    q_src[z, x, :, 0, :] = slope[32 * z + 8 * x : 32 * z + 8 * x + 8, :]
            begin(slope_hops[0])

    lasts = [i for i, step in enumerate(PLAN) if step[0] == "R"][-2:]
    for i, step in enumerate(PLAN):
        kind = step[0]
        if step == "bar":
            pl.semaphore_wait(pltpu.get_barrier_semaphore(), 13)
        elif step == "stat":
            norm_statistics()
        elif step == "cot":
            cotangents()
        elif step == "table":
            cotangent_table()
        elif kind == "A":
            hidden_inputs(int(step[1]))
        elif kind == "B":
            slopes(int(step[1]))
        elif kind == "D":
            rest(int(step[1]))
        else:
            c, d = int(step[1]), step[2]
            done = hops.setdefault((kind, c), [])
            k = len(done)
            bufs = families[kind]
            if k:
                done[-1].arrived()
            elif kind == "T":
                pack(index_ref, c // 2, table_ref, c % 2, t_src.at[c])
            elif kind == "C":
                pack(index_ref, c // 2, cot_table, c % 2, c_src.at[c])
            n = "TCR".index(kind) * 8 + c
            hop = Hop(
                d, AXIS[d], bufs[k].at[c], bufs[k + 1].at[c],
                (ssem.at[n, k], rsem.at[n, k], lsem.at[n, k]),
            )
            begin(hop)
            done.append(hop)
            if i == lasts[0]:
                slope_hops[0].arrived()
                begin(slope_hops[1])
    slope_hops[1].arrived()
    begin(slope_hops[2])
    for c in range(8):
        hops["R", c][2].arrived()
    slope_hops[2].arrived()
    for hop in every:
        hop.left()


def finish_kernel(spot_ref, back_ref, slope_ref, pick_ref, token_ref, gates_ref, sums):
    def body(i, carry):
        for j in range(8):
            t = i * 8 + j
            for h in range(2):
                one = back_ref[spot_ref[0, t] + 128 * h].astype(F32)
                two = back_ref[spot_ref[1, t] + 128 * h].astype(F32)
                sums[h, t] = (one + two).astype(BF16)
        return carry

    lax.fori_loop(0, 16, body, 0)
    perm = to_rows()
    for h in range(2):

        def put(g, b, rows, h=h):
            token_ref[32 * g : 32 * (g + 1), 1024 * h + 128 * b : 1024 * h + 128 * (b + 1)] = rows

        row_pair(perm, lambda g, h=h: sums[h, 32 * g : 32 * (g + 1)].reshape(256, 128), put)
    slope = slope_ref[:, 0, :].astype(BF16)
    pick = pick_ref[...]
    lane = iota((128, 128), 1)
    lane_f = lane.astype(F32)
    both = jnp.zeros((128, 128), F32)
    for k in range(2):
        one = (pick[:, 2 + k : 3 + k] == lane_f).astype(F32).astype(BF16)
        mine = jnp.where(lane_f == pick[:, 4 + k : 5 + k], dot(one, slope), 0.0)
        both = jnp.where(lane == k, jnp.sum(mine, axis=1, keepdims=True), both)
    gates_ref[...] = both.T[:2].astype(BF16)


def struct(shape, dtype=BF16):
    return jax.ShapeDtypeStruct(shape, dtype)


def local(tokens, routes, gates, w_gate, w_up, w_down, moe_out, norm_gain, out_grad):
    gain = norm_gain.reshape(1, 256)
    index, spot, gate, pick, table, stat = pl.pallas_call(
        route_kernel,
        out_shape=(
            struct((8, 128), jnp.int32),
            struct((8, 128), jnp.int32),
            struct((128, 1, 128), F32),
            struct((128, 128), F32),
            struct((2, 129, 8, 128)),
            struct((2, 8, 128), F32),
        ),
        in_specs=[VMEM] * 6,
        out_specs=(VMEM,) * 6,
        name="route",
    )(routes.T, gates.T, tokens, moe_out, out_grad, gain)
    pieces = (8, 4, 4, 8, 8, 128)
    lanes = (4, 4, 8, 1, 128)
    back, slope, x_rows, d_gate, d_up, hidden, scaled_cot = pl.pallas_call(
        mega_kernel,
        out_shape=(
            struct(pieces),
            struct(lanes, F32),
            struct((512, 2048)),
            struct((512, 768)),
            struct((512, 768)),
            struct((512, 768)),
            struct((512, 2048)),
        ),
        in_specs=[SMEM] + [VMEM] * 6 + [ANY] * 3,
        out_specs=(VMEM,) * 7,
        scratch_shapes=[
            pltpu.VMEM((2048, 768), BF16),
            pltpu.VMEM((2048, 768), BF16),
            pltpu.VMEM((768, 2048), BF16),
            *[pltpu.VMEM(pieces, BF16)] * 11,
            *[pltpu.VMEM(lanes, F32)] * 6,
            pltpu.VMEM((8, 2, 8, 128), F32),
            pltpu.VMEM((8, 128, 256), BF16),
            pltpu.VMEM((8, 128, 256), BF16),
            pltpu.VMEM((2, 129, 8, 128), BF16),
            pltpu.VMEM((4, 128, 768), F32),
            pltpu.VMEM((4, 128, 768), F32),
            pltpu.VMEM((128, 2048), BF16),
            pltpu.VMEM((128, 1024), BF16),
            pltpu.VMEM((128, 128), F32),
            pltpu.SemaphoreType.DMA((24, 3)),
            pltpu.SemaphoreType.DMA((24, 3)),
            pltpu.SemaphoreType.DMA((24, 3)),
            pltpu.SemaphoreType.DMA((8, 3)),
            pltpu.SemaphoreType.DMA((3,)),
        ],
        compiler_params=pltpu.CompilerParams(
            collective_id=0, has_side_effects=True, vmem_limit_bytes=62 << 20
        ),
        name="exchange",
    )(index, gate.reshape(lanes), table, stat, moe_out, out_grad, gain, w_gate[0], w_up[0], w_down[0])
    token_grad, gates_grad = pl.pallas_call(
        finish_kernel,
        out_shape=(struct((128, 2048)), struct((2, 128))),
        in_specs=[SMEM] + [VMEM] * 3,
        out_specs=(VMEM,) * 2,
        scratch_shapes=[pltpu.VMEM((2, 128, 8, 128), BF16)],
        name="finish",
    )(spot, back.reshape(1024, 8, 128), slope.reshape(128, 1, 128), pick)
    grads = [
        dot(a, b, 0, 0).astype(BF16)[None]
        for a, b in ((x_rows, d_gate), (x_rows, d_up), (hidden, scaled_cot))
    ]
    return (token_grad, gates_grad.T, *grads)


def solution(mesh):
    split = P(("ep", "tp"), None)
    expert = P(("ep", "tp"), None, None)
    in_specs = (split, split, split, expert, expert, expert, P("ep", "tp"), P("tp"), P("ep", "tp"))
    out_specs = (split, split, expert, expert, expert)
    return jax.shard_map(local, mesh=mesh, in_specs=in_specs, out_specs=out_specs, check_vma=False)
```

time: 209 us -> 123 us (0.59)
  Pallas kernels: 0 us -> 110 us
  waiting for transfers between devices: 63.6 us -> 0 us
  local copies, waits for them, and re-layouts: 61.4 us -> 0.02 us
  starting transfers between devices: 37.5 us -> 0 us
  matrix products: 31.3 us -> 12.5 us
  other arithmetic: 12.6 us -> 0 us
    pallas_call x0 -> x3, Pallas kernels: none -> 110 us  [the longest x1 103 us: local(): pl.pallas_call(mega_kernel, out_shape=(struct(pieces), struct(lanes, F32)...]
    all_to_all x6 -> x0, waiting for transfers between devices: 63.6 us -> none  [the longest x1 20.1 us: local(): lax.all_to_all(cot_slots, ('ep', 'tp'), split_axis=0, concat_axis=0, tile...]
    all_to_all x6 -> x0, starting transfers between devices: 37.5 us -> none  [the longest x1 10.3 us: local(): lax.all_to_all(gate_slots, ('ep', 'tp'), split_axis=0, concat_axis=0, til...]
    reshape x7 -> x0, local copies, waits for them, and re-layouts: 22.9 us -> none  [the longest x1 4.09 us: local(): cot_slots = cot_pad[token_of_slot].reshape(devices, capacity, features)]
    gather x5 -> x0, local copies, waits for them, and re-layouts: 22.5 us -> none  [the longest x2 7.88 us: local(): per_route = back_rows.reshape(devices * capacity, features)[own_slots]]
    dot_general x8 -> x3, matrix products: 31.3 us -> 12.5 us  [dot(): lax.dot_general(a, b, (((a_dim,), (b_dim,)), ((), ())), preferred_element...]
    reduce_sum x4 -> x0, other arithmetic: 6.51 us -> none  [the longest x1 4.57 us: local(): jnp.sum(per_route.astype(jnp.float32).reshape(tok_rows, top_count, featur...]
    split x2 -> x0, local copies, waits for them, and re-layouts: 3.64 us -> none  [sent_together(): jnp.split(result, [sum(widths[:k]) for k in range(1, len(widths))], axis=...]
  transfers between devices with their start and end apart: 6 -> 0, of which waited for: 4 -> 0; matrix products, arithmetic and copies ran while one was open for 27% -> 0% of each run, Pallas kernels for 0% -> 0%
where the time goes in v1:
time: 123 us
  Pallas kernels  110 us (89%)
  matrix products  12.5 us (10%)
    pallas_call x1, Pallas kernels, local(): pl.pallas_call(mega_kernel, out_shape=(struct(pieces), struct(lanes, F32)...  103 us
    dot_general x3, matrix products, dot(): lax.dot_general(a, b, (((a_dim,), (b_dim,)), ((), ())), preferred_element...  12.5 us
    pallas_call x1, Pallas kernels, local(): pl.pallas_call(finish_kernel, out_shape=(struct((128, 2048)), struct((2,...  3.5 us
    pallas_call x1, Pallas kernels, local(): pl.pallas_call(route_kernel, out_shape=(struct((8, 128), jnp.int32), stru...  3.15 us

profile of v1, /device:TPU:1, one launch (start us, length us, event | category | flops | bytes accessed | tf_op | source)
XLA Modules:
  0.0 122.6 jit_solution(11726186728962984233)
XLA Ops:
  0.6 3.2 %route.1 = (s32[8,128]{1,0:T(8,128)}, s32[8,128]{1,0:T(8,128)}, f32[128,1,128]{2,1,0:T(1,128)}, f32[128,128]{1,0:T(8,128)}, bf16[2,129,8,128]{3,2,1,0:T(8,128)(2,1)}, /*index=5*/f32[2,8,128]{2,1,0:T(8,128)}) custom-call(s32[2,128]{1,0:T(2,128)} %bitcast.30, f32[2,128]{1,0:T(2,128)} %bitcast.31, bf16[128,2048]{1,0:T(8,128)(2,1)} %tokens_ref.1, ...), custom_call_target="tpu_custom_call" | custom-call | tf_op jit(solution)/shard_map/route/pallas_call | solution.py:456
  3.8 102.8 %exchange.1 = (bf16[8,4,4,8,8,128]{5,4,3,2,1,0:T(8,128)(2,1)}, f32[4,4,8,1,128]{4,3,2,1,0:T(1,128)}, bf16[512,2048]{1,0:T(8,128)(2,1)}, bf16[512,768]{1,0:T(8,12...) custom-call(s32[8,128]{1,0:T(8,128)} %get-tuple-element.21.index_ref, ...), custom_call_target="tpu_custom_call" | custom-call | tf_op jit(solution)/shard_map/exchange/pallas_call | solution.py:472
  106.6 3.5 %finish.1 = (bf16[128,2048]{1,0:T(8,128)(2,1)}, bf16[2,128]{1,0:T(2,128)(2,1)}) custom-call(s32[8,128]{1,0:T(8,128)} %get-tuple-element.20.spot_ref, bf16[1024,8,128]{2,1,0:T(8,128)(2,1)} %bitcast.25, f32[128,1,128]{2,1,0:T(1,128)} %bitcast.27, f32[128,128]{1,0:T(8,128)} %get-tuple-element.27.pick_ref), custom_call_target="tpu_custom_call" | custom-call | tf_op jit(solution)/shard_map/finish/pallas_call | solution.py:511
  110.1 0.0 copy-start.1
  110.1 0.0 copy-start.3
  110.1 5.4 %fusion = bf16[1,2048,768]{2,1,0:T(8,128)(2,1)} fusion(bf16[512,2048]{1,0:T(8,128)(2,1)} %get-tuple-element.30, bf16[512,768]{1,0:T(8,128)(2,1)} %get-tuple-element.31), kind=kOutput, calls=%fused_computation.3 | convolution fusion | flops 1612185600 | bytes 6029312 | tf_op jit(solution)/shard_map/dot_general | solution.py:35
  115.6 0.0 copy-done.1
  115.6 0.0 copy-done.3
  115.6 0.0 copy-start
  115.6 0.0 copy-start.2
  115.6 3.5 %fusion.1 = bf16[1,2048,768]{2,1,0:T(8,128)(2,1)} fusion(bf16[512,2048]{1,0:T(8,128)(2,1)S(1)} %copy-done.1, bf16[512,768]{1,0:T(8,128)(2,1)S(1)} %copy-done.3), kind=kOutput, calls=%fused_computation.4 | convolution fusion | flops 1612185600 | bytes 6029312 | tf_op jit(solution)/shard_map/dot_general | solution.py:35
  119.1 0.0 copy-done
  119.1 0.0 copy-done.2
  119.1 3.5 %fusion.2 = bf16[1,768,2048]{2,1,0:T(8,128)(2,1)} fusion(bf16[512,768]{1,0:T(8,128)(2,1)S(1)} %copy-done.2, bf16[512,2048]{1,0:T(8,128)(2,1)S(1)} %copy-done), kind=kOutput, calls=%fused_computation.5 | convolution fusion | flops 1612185600 | bytes 6029312 | tf_op jit(solution)/shard_map/dot_general | solution.py:35
Async XLA Ops:
  110.1 5.4 %copy-start.1 = (bf16[512,2048]{1,0:T(8,128)(2,1)S(1)}, bf16[512,2048]{1,0:T(8,128)(2,1)}, u32[]{:S(2)}) copy-start(bf16[512,2048]{1,0:T(8,128)(2,1)} %get-tuple-element.30) | copy-start | bytes 6291460
  110.1 5.4 %copy-start.3 = (bf16[512,768]{1,0:T(8,128)(2,1)S(1)}, bf16[512,768]{1,0:T(8,128)(2,1)}, u32[]{:S(2)}) copy-start(bf16[512,768]{1,0:T(8,128)(2,1)} %get-tuple-element.32) | copy-start | bytes 2359300
  115.6 3.6 %copy-start = (bf16[512,2048]{1,0:T(8,128)(2,1)S(1)}, bf16[512,2048]{1,0:T(8,128)(2,1)}, u32[]{:S(2)}) copy-start(bf16[512,2048]{1,0:T(8,128)(2,1)} %get-tuple-element.34) | copy-start | bytes 6291460
  115.6 3.6 %copy-start.2 = (bf16[512,768]{1,0:T(8,128)(2,1)S(1)}, bf16[512,768]{1,0:T(8,128)(2,1)}, u32[]{:S(2)}) copy-start(bf16[512,768]{1,0:T(8,128)(2,1)} %get-tuple-element.33) | copy-start | bytes 2359300

commit v2 on v1

--- a/solution.py
+++ b/solution.py
@@ -16,14 +16,15 @@
 epsilon = 1e-06
 
 PLAN = (
-    "bar", "T1t", "T0x", "stat", "T7x", "T4z", "T5z", "T2t", "cot", "T3x", "T1z", "T4x",
-    "T7z", "T0z", "T2x", "T6t", "T1x", "T5t", "T3z", "table", "C0t", "C1x", "T4t", "C3t",
-    "T2z", "C2x", "C4z", "C7x", "T3t", "C1z", "C0x", "C6t", "C2z", "T0t", "T5x", "C3z",
-    "C5x", "C1t", "T6z", "C0z", "C6x", "C2t", "A1", "C3x", "C4x", "A2", "T6x", "C7z",
-    "C5t", "T7t", "A0", "C6z", "B0", "D0", "R1z", "C7t", "B1", "C5z", "R2x", "R0x",
-    "C4t", "D1", "R3z", "A3", "R1t", "B3", "R6z", "R2t", "B2", "R4z", "R0t", "R1x",
-    "D2", "R3x", "R5z", "D3", "R7t", "R6x", "R2z", "R4t", "R5x", "R7z", "R3t", "R0z",
-    "R6t", "R4x", "R7x", "R5t",
+    "bar", "stat", "T7z", "T2x", "T0t", "T1x", "T5x", "T6z", "cot", "M0", "M2", "T3z",
+    "T4x", "T1t", "T6x", "T2t", "T0z", "table", "C0z", "C1t", "C5z", "T0x", "C3x", "C2z",
+    "C6t", "C7z", "T1z", "C0t", "C1x", "T3t", "C6x", "C2t", "C3t", "C1z", "C0x", "C7x",
+    "T7t", "C4z", "T4t", "M1", "T3x", "A0", "T6t", "T2z", "C3z", "T5z", "C2x", "B0",
+    "C5t", "T7x", "C4x", "D0", "R1x", "A1", "C6z", "T4z", "R0x", "C7t", "B1", "R2z",
+    "T5t", "A3", "C4t", "D1", "R3t", "C5x", "B3", "R1z", "D3", "R7x", "R0z", "R6t",
+    "R2t", "A2", "B2", "R4t", "D2", "R5x", "R7z", "S0", "R6x", "R0t", "R3z", "S3",
+    "W0", "W4", "R1t", "S1", "W1", "S2", "W9", "R4x", "R5z", "R2x", "R7t", "W10",
+    "W8", "W6", "R6z", "R3x", "R4z", "R5t", "W7", "W2", "W5", "W3",
 )
 
 
@@ -66,10 +67,17 @@
                 put(2 * pair + j, b, out[32 * b : 32 * (b + 1), 128 * j : 128 * (j + 1)])
 
 
-def route_kernel(
-    routes_ref, gates_ref, tokens_ref, moe_ref, grad_ref, gain_ref,
-    index_ref, spot_ref, gate_ref, pick_ref, table_ref, stat_ref,
-):
+def statistics(moe, grad, gain_ref, stat_ref):
+    for b in range(8):
+        rows = slice(128 * b, 128 * (b + 1))
+        saved = moe[rows, :].astype(F32)
+        scaled = gain_ref[...] * grad[rows, :].astype(F32)
+        for s, prod in enumerate((saved * saved, saved * scaled)):
+            part = (prod[:, :128] + prod[:, 128:]).T
+            stat_ref[s, b : b + 1, :] = jnp.sum(part, axis=0, keepdims=True)
+
+
+def routing(routes_ref, gates_ref, index_ref, spot_ref, gate_ref, pick_ref):
     head = jnp.concatenate(
         [routes_ref[...].astype(F32), gates_ref[...], jnp.zeros((4, 128), F32)], axis=0
     )
@@ -88,8 +96,10 @@
         one = hot[k].astype(BF16)
         index += dot(jnp.where(at, number, 0.0).astype(BF16), one, 0, 0)
         gate += dot(one, jnp.where(at, cols[:, 2 + k : 3 + k], 0.0).astype(BF16), 0, 0)
-    index_ref[...] = index[:8].astype(jnp.int32)
-    gate_ref[:, 0, :] = gate
+    index_ref[...] = jnp.clip(index[:8].astype(jnp.int32), 0, 128)
+    for z in range(4):
+        for x in range(4):
+            gate_ref[z, x, :, 0, :] = gate[32 * z + 8 * x : 32 * z + 8 * x + 8, :]
     pick = jnp.zeros((128, 128), F32)
     for k in range(2):
         pick = jnp.where(lane == k, rank[k] * 256.0 + cols[:, k : k + 1], pick)
@@ -97,13 +107,15 @@
         pick = jnp.where(lane == 4 + k, rank[k], pick)
     pick_ref[...] = pick
     spot_ref[...] = pick.T[:8].astype(jnp.int32)
-    perm = to_tiles()
+
+
+def token_table(perm, tokens, table_ref):
     for h in range(2):
         table_ref[h, 0] = jnp.zeros((8, 128), BF16)
 
         def pieces(g, h=h):
             return [
-                tokens_ref[32 * g : 32 * (g + 1), 1024 * h + 128 * b : 1024 * h + 128 * (b + 1)]
+                tokens[32 * g : 32 * (g + 1), 1024 * h + 128 * b : 1024 * h + 128 * (b + 1)]
                 for b in range(8)
             ]
 
@@ -111,12 +123,6 @@
             table_ref[h, 1 + 32 * g : 33 + 32 * g] = tiles.reshape(32, 8, 128)
 
         tile_pair(perm, pieces, put)
-    for b in range(8):
-        saved = moe_ref[128 * b : 128 * (b + 1), :].astype(F32)
-        scaled = gain_ref[...] * grad_ref[128 * b : 128 * (b + 1), :].astype(F32)
-        for s, prod in enumerate((saved * saved, saved * scaled)):
-            part = (prod[:, :128] + prod[:, 128:]).T
-            stat_ref[s, b : b + 1, :] = jnp.sum(part, axis=0, keepdims=True)
 
 
 def coords():
@@ -154,7 +160,7 @@
 
 class Hop:
     def __init__(self, dim, axis, src, dst, sems, whole=False):
-        self.dim, self.axis, self.whole = dim, axis, whole
+        self.dim, self.axis, self.whole, self.gone = dim, axis, whole, False
         self.src, self.dst, (self.ssem, self.rsem, self.lsem) = src, dst, sems
 
     def piece(self, index):
@@ -184,6 +190,9 @@
         pltpu.make_async_copy(one, one, self.lsem).wait()
 
     def left(self):
+        if self.gone:
+            return
+        self.gone = True
         part = self.remote_part()
         pltpu.make_async_copy(part, part, self.ssem).wait()
 
@@ -198,26 +207,49 @@
 
 
 def mega_kernel(
-    index_ref, gate_ref, table_ref, stat_ref, moe_ref, grad_ref, gain_ref, wg_any, wu_any, wd_any,
-    back_ref, slope_ref, x_rows, d_gate, d_up, hidden, scaled_cot,
-    wg, wu, wd, t_src, t_one, t_two, t_out, c_src, c_one, c_two, c_out, r_src, r_one, r_two,
+    routes_ref, gates_ref, gain_ref, tokens_any, moe_any, grad_any, wg_any, wu_any, wd_any,
+    back_ref, slope_ref, spot_ref, pick_ref, gate_grad, up_grad, down_grad,
+    tokens, moe, grad, index_v, index_ref, gate_src, table_ref, stat_ref,
+    wg_t, wu_t, wd_t, t_src, t_one, t_two, t_out, c_src, c_one, c_two, c_out, r_one, r_two,
     g_one, g_two, g_out, q_src, q_one, q_two, s_in, cot_out, cot_in, cot_table,
-    pre_gate, pre_up, cot_rows, back_rows, slope,
+    x_rows, x_t, d_gate, d_up, hidden, pre_gate, pre_up, cot_rows, back_rows, slope,
     ssem, rsem, lsem, misc, wsem,
 ):
+    wg, wu = gate_grad, up_grad
+    loads = [
+        pltpu.make_async_copy(a, b, wsem.at[i])
+        for i, (a, b) in enumerate(
+            (
+                (moe_any, moe), (grad_any, grad), (tokens_any, tokens),
+                (wg_any, gate_grad), (wu_any, up_grad), (wd_any, down_grad),
+            )
+        )
+    ]
+    loaded = set()
+
+    def need(*which):
+        for i in which:
+            if i not in loaded:
+                loads[i].wait()
+                loaded.add(i)
+
+    for load in loads:
+        load.start()
     greet()
-    weights = [
-        pltpu.make_async_copy(a, b, wsem.at[i])
-        for i, (a, b) in enumerate(((wg_any, wg), (wu_any, wu), (wd_any, wd)))
-    ]
-    for w in weights:
-        w.start()
     slope[...] = jnp.zeros((128, 128), F32)
     unpack_perm, pack_perm = to_rows(), to_tiles()
+    routing(routes_ref, gates_ref, index_v, spot_ref, gate_src, pick_ref)
+    index_copy = pltpu.make_async_copy(index_v, index_ref, wsem.at[6])
+    index_copy.start()
+    need(0, 1)
+    statistics(moe, grad, gain_ref, stat_ref)
+    need(2)
+    token_table(pack_perm, tokens, table_ref)
+    index_copy.wait()
     families = {
         "T": (t_src, t_one, t_two, t_out),
         "C": (c_src, c_one, c_two, c_out),
-        "R": (r_src, r_one, r_two, back_ref),
+        "R": (t_src, r_one, r_two, back_ref),
     }
     hops = {}
     every = []
@@ -230,7 +262,7 @@
     gate_hops = [
         Hop(d, AXIS[d], a, b, small(2 + i))
         for i, (d, a, b) in enumerate(
-            (("x", gate_ref, g_one), ("t", g_one, g_two), ("z", g_two, g_out))
+            (("x", gate_src, g_one), ("t", g_one, g_two), ("z", g_two, g_out))
         )
     ]
     slope_hops = [
@@ -258,8 +290,8 @@
 
         for b in range(8):
             rows = slice(128 * b, 128 * (b + 1))
-            scaled = gain_ref[...] * grad_ref[rows, :].astype(F32)
-            saved = moe_ref[rows, :].astype(F32)
+            scaled = gain_ref[...] * grad[rows, :].astype(F32)
+            saved = moe[rows, :].astype(F32)
             cot_out[b] = (
                 cols[:, b : b + 1] * scaled - saved * cols[:, 8 + b : 9 + b]
             ).astype(BF16)
@@ -294,32 +326,39 @@
         row_pair(unpack_perm, lambda g: src[g].reshape(256, 128), put)
 
     def hidden_inputs(r):
-        if r == 1:
-            weights[0].wait()
-            weights[1].wait()
+        need(3, 4)
         for h in range(2):
             hops["T", 2 * r + h][2].arrived()
-            unpack(t_out.at[2 * r + h], x_rows, 128 * r, h)
+            unpack(t_out.at[2 * r + h], x_rows, 0, h)
 
         def body(n, carry):
             cols = pl.ds(pl.multiple_of(n * 256, 256), 256)
-            x = x_rows[128 * r : 128 * (r + 1), :]
+            x = x_rows[...]
             pre_gate[r, :, cols] = dot(x, wg[:, cols])
             pre_up[r, :, cols] = dot(x, wu[:, cols])
             return carry
 
         lax.fori_loop(0, 3, body, 0)
 
+        def turned(n, carry):
+            cols = pl.ds(pl.multiple_of(n * 256, 256), 256)
+            x_t[cols, 128 * r : 128 * (r + 1)] = x_rows[:, cols].T
+            return carry
+
+        lax.fori_loop(0, 8, turned, 0)
+
     def half_back(r, h):
         rows = slice(128 * r, 128 * (r + 1))
 
         def body(n, carry):
-            wide = pl.ds(pl.multiple_of(1024 * h + n * 256, 256), 256)
-            total = dot(d_gate[rows, :], wg[wide, :], 1, 1) + dot(d_up[rows, :], wu[wide, :], 1, 1)
-            back_rows[:, pl.ds(pl.multiple_of(n * 256, 256), 256)] = total.astype(BF16)
+            wide = pl.ds(pl.multiple_of(1024 * h + n * 512, 512), 512)
+            total = dot(d_gate[rows, :], wg_t[:, wide]) + dot(d_up[rows, :], wu_t[:, wide])
+            back_rows[:, pl.ds(pl.multiple_of(n * 512, 512), 512)] = total.astype(BF16)
             return carry
 
-        lax.fori_loop(0, 4, body, 0)
+        lax.fori_loop(0, 2, body, 0)
+
+        hops["T", 2 * r + h][0].left()
 
         def pieces(g):
             return [
@@ -327,26 +366,28 @@
             ]
 
         def put(g, tiles):
-            r_src[2 * r + h, g] = tiles.reshape(4, 8, 8, 128)
+            t_src[2 * r + h, g] = tiles.reshape(4, 8, 8, 128)
 
         tile_pair(pack_perm, pieces, put)
+
+    def gate_of(r):
+        gates = jnp.concatenate(
+            [g_out[z, x][:, 0, :] for z in range(4) for x in range(4)], axis=0
+        )
+        return gates[:, r : r + 1]
 
     def slopes(r):
         if r == 0:
-            weights[2].wait()
             gate_hops[2].arrived()
         for h in range(2):
             hops["C", 2 * r + h][2].arrived()
-            unpack(c_out.at[2 * r + h], cot_rows, 0, h)
-        gates = jnp.concatenate(
-            [g_out[z, x][:, 0, :] for z in range(4) for x in range(4)], axis=0
-        )
-        gate = gates[:, r : r + 1]
+            unpack(c_out.at[2 * r + h], cot_rows, 128 * r, h)
+        gate = gate_of(r)
         rows = slice(128 * r, 128 * (r + 1))
 
         def body(n, carry):
             cols = pl.ds(pl.multiple_of(n * 256, 256), 256)
-            hid_grad = dot(cot_rows[...], wd[cols, :], 1, 1)
+            hid_grad = dot(cot_rows[rows, :], wd_t[:, cols])
             p_gate, p_up = pre_gate[r, :, cols], pre_up[r, :, cols]
             sig = jax.nn.sigmoid(p_gate)
             act = p_gate * sig
@@ -359,18 +400,54 @@
 
         total = lax.fori_loop(0, 3, body, jnp.zeros((128, 1), F32))
         slope[...] = jnp.where(iota((128, 128), 1) == r, total, slope[...])
-        scaled_cot[rows, :] = (gate * cot_rows[...].astype(F32)).astype(BF16)
         half_back(r, 0)
 
     def rest(r):
         half_back(r, 1)
-        if r == 3:
+        if r == 2:
             for z in range(4):
                 for x in range(4):
                     q_src[z, x, :, 0, :] = slope[32 * z + 8 * x : 32 * z + 8 * x + 8, :]
             begin(slope_hops[0])
 
-    lasts = [i for i, step in enumerate(PLAN) if step[0] == "R"][-2:]
+    def turn(src, dst):
+        def body(n, carry):
+            rows = pl.ds(pl.multiple_of(n * 256, 256), 256)
+            dst[:, rows] = src[rows, :].T
+            return carry
+
+        lax.fori_loop(0, src.shape[0] // 256, body, 0)
+
+    def turn_weight(i):
+        if i == 0:
+            need(5)
+            turn(down_grad, wd_t)
+        elif i == 1:
+            need(3)
+            turn(gate_grad, wg_t)
+        else:
+            need(4)
+            turn(up_grad, wu_t)
+
+    def scale(r):
+        rows = slice(128 * r, 128 * (r + 1))
+        cot_rows[rows, :] = (gate_of(r) * cot_rows[rows, :].astype(F32)).astype(BF16)
+
+    def weight_grad(i):
+        if i >= 8:
+            rows = slice(256 * (i - 8), 256 * (i - 7))
+            down_grad[rows, :] = dot(hidden[:, rows], cot_rows[...], 0, 0).astype(BF16)
+            return
+        out, right = ((gate_grad, d_gate), (up_grad, d_up))[i // 4]
+
+        def body(n, carry):
+            rows = pl.ds(pl.multiple_of(512 * (i % 4) + n * 256, 256), 256)
+            out[rows, :] = dot(x_t[rows, :], right[...]).astype(BF16)
+            return carry
+
+        lax.fori_loop(0, 2, body, 0)
+
+    lasts = (86, 98)
     for i, step in enumerate(PLAN):
         kind = step[0]
         if step == "bar":
@@ -387,6 +464,12 @@
             slopes(int(step[1]))
         elif kind == "D":
             rest(int(step[1]))
+        elif kind == "M":
+            turn_weight(int(step[1]))
+        elif kind == "S":
+            scale(int(step[1]))
+        elif kind == "W":
+            weight_grad(int(step[1:]))
         else:
             c, d = int(step[1]), step[2]
             done = hops.setdefault((kind, c), [])
@@ -405,11 +488,9 @@
             )
             begin(hop)
             done.append(hop)
-            if i == lasts[0]:
-                slope_hops[0].arrived()
-                begin(slope_hops[1])
-    slope_hops[1].arrived()
-    begin(slope_hops[2])
+            if i in (lasts[0], lasts[1]):
+                slope_hops[lasts.index(i)].arrived()
+                begin(slope_hops[lasts.index(i) + 1])
     for c in range(8):
         hops["R", c][2].arrived()
     slope_hops[2].arrived()
@@ -417,7 +498,19 @@
         hop.left()
 
 
-def finish_kernel(spot_ref, back_ref, slope_ref, pick_ref, token_ref, gates_ref, sums):
+def finish_kernel(
+    spot_ref, back_ref, slope_ref, pick_ref, gate_grad, up_grad, down_grad,
+    token_ref, gates_ref, gate_out, up_out, down_out, sums, sem,
+):
+    copies = [
+        pltpu.make_async_copy(a, b.at[0], sem.at[i])
+        for i, (a, b) in enumerate(
+            ((gate_grad, gate_out), (up_grad, up_out), (down_grad, down_out))
+        )
+    ]
+    for copy in copies:
+        copy.start()
+
     def body(i, carry):
         for j in range(8):
             t = i * 8 + j
@@ -445,6 +538,8 @@
         mine = jnp.where(lane_f == pick[:, 4 + k : 5 + k], dot(one, slope), 0.0)
         both = jnp.where(lane == k, jnp.sum(mine, axis=1, keepdims=True), both)
     gates_ref[...] = both.T[:2].astype(BF16)
+    for copy in copies:
+        copy.wait()
 
 
 def struct(shape, dtype=BF16):
@@ -452,74 +547,80 @@
 
 
 def local(tokens, routes, gates, w_gate, w_up, w_down, moe_out, norm_gain, out_grad):
-    gain = norm_gain.reshape(1, 256)
-    index, spot, gate, pick, table, stat = pl.pallas_call(
-        route_kernel,
-        out_shape=(
-            struct((8, 128), jnp.int32),
-            struct((8, 128), jnp.int32),
-            struct((128, 1, 128), F32),
-            struct((128, 128), F32),
-            struct((2, 129, 8, 128)),
-            struct((2, 8, 128), F32),
-        ),
-        in_specs=[VMEM] * 6,
-        out_specs=(VMEM,) * 6,
-        name="route",
-    )(routes.T, gates.T, tokens, moe_out, out_grad, gain)
     pieces = (8, 4, 4, 8, 8, 128)
     lanes = (4, 4, 8, 1, 128)
-    back, slope, x_rows, d_gate, d_up, hidden, scaled_cot = pl.pallas_call(
+    deep, flat = (2048, 768), (768, 2048)
+    rows, inner = (512, 2048), (512, 768)
+    back, slope, spot, pick, gate_grad, up_grad, down_grad = pl.pallas_call(
         mega_kernel,
         out_shape=(
-            struct(pieces),
-            struct(lanes, F32),
-            struct((512, 2048)),
-            struct((512, 768)),
-            struct((512, 768)),
-            struct((512, 768)),
-            struct((512, 2048)),
+            pltpu.VMEM(pieces, BF16),
+            pltpu.VMEM(lanes, F32),
+            struct((8, 128), jnp.int32),
+            pltpu.VMEM((128, 128), F32),
+            pltpu.VMEM(deep, BF16),
+            pltpu.VMEM(deep, BF16),
+            pltpu.VMEM(flat, BF16),
         ),
-        in_specs=[SMEM] + [VMEM] * 6 + [ANY] * 3,
+        in_specs=[VMEM] * 3 + [ANY] * 6,
         out_specs=(VMEM,) * 7,
         scratch_shapes=[
-            pltpu.VMEM((2048, 768), BF16),
-            pltpu.VMEM((2048, 768), BF16),
-            pltpu.VMEM((768, 2048), BF16),
-            *[pltpu.VMEM(pieces, BF16)] * 11,
+            pltpu.VMEM((128, 2048), BF16),
+            pltpu.VMEM((1024, 256), BF16),
+            pltpu.VMEM((1024, 256), BF16),
+            pltpu.VMEM((8, 128), jnp.int32),
+            pltpu.SMEM((8, 128), jnp.int32),
+            pltpu.VMEM(lanes, F32),
+            pltpu.VMEM((2, 129, 8, 128), BF16),
+            pltpu.VMEM((2, 8, 128), F32),
+            pltpu.VMEM(flat, BF16),
+            pltpu.VMEM(flat, BF16),
+            pltpu.VMEM(deep, BF16),
+            *[pltpu.VMEM(pieces, BF16)] * 10,
             *[pltpu.VMEM(lanes, F32)] * 6,
             pltpu.VMEM((8, 2, 8, 128), F32),
             pltpu.VMEM((8, 128, 256), BF16),
             pltpu.VMEM((8, 128, 256), BF16),
             pltpu.VMEM((2, 129, 8, 128), BF16),
+            pltpu.VMEM((128, 2048), BF16),
+            pltpu.VMEM((2048, 512), BF16),
+            pltpu.VMEM(inner, BF16),
+            pltpu.VMEM(inner, BF16),
+            pltpu.VMEM(inner, BF16),
             pltpu.VMEM((4, 128, 768), F32),
             pltpu.VMEM((4, 128, 768), F32),
-            pltpu.VMEM((128, 2048), BF16),
+            pltpu.VMEM(rows, BF16),
             pltpu.VMEM((128, 1024), BF16),
             pltpu.VMEM((128, 128), F32),
             pltpu.SemaphoreType.DMA((24, 3)),
             pltpu.SemaphoreType.DMA((24, 3)),
             pltpu.SemaphoreType.DMA((24, 3)),
             pltpu.SemaphoreType.DMA((8, 3)),
-            pltpu.SemaphoreType.DMA((3,)),
+            pltpu.SemaphoreType.DMA((7,)),
         ],
         compiler_params=pltpu.CompilerParams(
-            collective_id=0, has_side_effects=True, vmem_limit_bytes=62 << 20
+            collective_id=0, has_side_effects=True, vmem_limit_bytes=46 << 20
         ),
         name="exchange",
-    )(index, gate.reshape(lanes), table, stat, moe_out, out_grad, gain, w_gate[0], w_up[0], w_down[0])
-    token_grad, gates_grad = pl.pallas_call(
+    )(
+        routes.T, gates.T, norm_gain.reshape(1, 256), tokens, moe_out, out_grad,
+        w_gate[0], w_up[0], w_down[0],
+    )
+    token_grad, gates_grad, *grads = pl.pallas_call(
         finish_kernel,
-        out_shape=(struct((128, 2048)), struct((2, 128))),
-        in_specs=[SMEM] + [VMEM] * 3,
-        out_specs=(VMEM,) * 2,
-        scratch_shapes=[pltpu.VMEM((2, 128, 8, 128), BF16)],
+        out_shape=(
+            struct((128, 2048)),
+            struct((2, 128)),
+            struct((1, *deep)),
+            struct((1, *deep)),
+            struct((1, *flat)),
+        ),
+        in_specs=[SMEM] + [VMEM] * 6,
+        out_specs=(VMEM, VMEM, ANY, ANY, ANY),
+        scratch_shapes=[pltpu.VMEM((2, 128, 8, 128), BF16), pltpu.SemaphoreType.DMA((3,))],
+        compiler_params=pltpu.CompilerParams(vmem_limit_bytes=8 << 20),
         name="finish",
-    )(spot, back.reshape(1024, 8, 128), slope.reshape(128, 1, 128), pick)
-    grads = [
-        dot(a, b, 0, 0).astype(BF16)[None]
-        for a, b in ((x_rows, d_gate), (x_rows, d_up), (hidden, scaled_cot))
-    ]
+    )(spot, back.reshape(1024, 8, 128), slope.reshape(128, 1, 128), pick, gate_grad, up_grad, down_grad)
     return (token_grad, gates_grad.T, *grads)
 
 

time: 123 us -> 96.7 us (0.79)
  Pallas kernels: 110 us -> 95.1 us
  matrix products: 12.5 us -> 0 us
    pallas_call x2 -> x1, Pallas kernels: 106 us -> 89.9 us  [local(): pl.pallas_call(mega_kernel, out_shape=(pltpu.VMEM(pieces, BF16), pltpu.VM...]
    dot_general x3 -> x0, matrix products: 12.5 us -> none  [dot(): lax.dot_general(a, b, (((a_dim,), (b_dim,)), ((), ())), preferred_element...]
    pallas_call x1, Pallas kernels: 3.5 us -> 5.15 us  [local(): pl.pallas_call(finish_kernel, out_shape=(struct((128, 2048)), struct((2,...]
where the time goes in v2:
time: 96.7 us; the launch traced here: 96.6 us
  Pallas kernels  95.1 us (98%)
    pallas_call x1, Pallas kernels, local(): pl.pallas_call(mega_kernel, out_shape=(pltpu.VMEM(pieces, BF16), pltpu.VM...  89.9 us
    pallas_call x1, Pallas kernels, local(): pl.pallas_call(finish_kernel, out_shape=(struct((128, 2048)), struct((2,...  5.15 us

profile of v2, /device:TPU:1, one launch (start us, length us, event | category | flops | bytes accessed | tf_op | source)
XLA Modules:
  0.0 96.6 jit_solution(10217182120564715835)
XLA Ops:
  0.6 89.9 %exchange.1 = (bf16[8,4,4,8,8,128]{5,4,3,2,1,0:T(8,128)(2,1)S(1)}, f32[4,4,8,1,128]{4,3,2,1,0:T(1,128)S(1)}, s32[8,128]{1,0:T(8,128)}, f32[128,128]{1,0:T(8,128)...) custom-call(s32[2,128]{1,0:T(2,128)} %bitcast.14, ...), custom_call_target="tpu_custom_call" | custom-call | tf_op jit(solution)/shard_map/exchange/pallas_call | solution.py:554
  90.6 0.0 copy-start
  90.6 0.7 copy-done
  91.2 5.2 %finish.1 = (bf16[128,2048]{1,0:T(8,128)(2,1)}, bf16[2,128]{1,0:T(2,128)(2,1)}, bf16[1,2048,768]{2,1,0:T(8,128)(2,1)}, bf16[1,2048,768]{2,1,0:T(8,128)(2,1)}, bf16[1,768,2048]{2,1,0:T(8,128)(2,1)}) custom-call(s32[8,128]{1,0:T(8,128)S(1)} %copy-done, bf16[1024,8,128]{2,1,0:T(8,128)(2,1)S(1)} %bitcast.9, f32[128,1,128]{2,1,0:T(1,128)S(1)} %bitcast.10, ...), custom_call_target="tpu_custom_call" | custom-call | tf_op jit(solution)/shard_map/finish/pallas_call | solution.py:609
Async XLA Ops:
  90.6 0.7 copy-start

commit v3 on v2

--- a/solution.py
+++ b/solution.py
@@ -16,15 +16,15 @@
 epsilon = 1e-06
 
 PLAN = (
-    "bar", "stat", "T7z", "T2x", "T0t", "T1x", "T5x", "T6z", "cot", "M0", "M2", "T3z",
-    "T4x", "T1t", "T6x", "T2t", "T0z", "table", "C0z", "C1t", "C5z", "T0x", "C3x", "C2z",
-    "C6t", "C7z", "T1z", "C0t", "C1x", "T3t", "C6x", "C2t", "C3t", "C1z", "C0x", "C7x",
-    "T7t", "C4z", "T4t", "M1", "T3x", "A0", "T6t", "T2z", "C3z", "T5z", "C2x", "B0",
-    "C5t", "T7x", "C4x", "D0", "R1x", "A1", "C6z", "T4z", "R0x", "C7t", "B1", "R2z",
-    "T5t", "A3", "C4t", "D1", "R3t", "C5x", "B3", "R1z", "D3", "R7x", "R0z", "R6t",
-    "R2t", "A2", "B2", "R4t", "D2", "R5x", "R7z", "S0", "R6x", "R0t", "R3z", "S3",
-    "W0", "W4", "R1t", "S1", "W1", "S2", "W9", "R4x", "R5z", "R2x", "R7t", "W10",
-    "W8", "W6", "R6z", "R3x", "R4z", "R5t", "W7", "W2", "W5", "W3",
+    "bar", "stat", "T3t", "T2z", "T0t", "T6x", "T1z", "T7z", "T4t", "T5x", "cot", "C0x",
+    "C1t", "C5z", "C2t", "T2x", "T0z", "T1t", "C7t", "M0", "T3x", "C3x", "C4t", "M1",
+    "C0z", "T5z", "C1x", "C2z", "T0x", "C0t", "T1x", "C3z", "C1z", "C6t", "M2", "T2t",
+    "T3z", "T4x", "C5x", "C3t", "C2x", "C4z", "T7t", "C7x", "T5t", "T6z", "A0", "B0",
+    "T4z", "A1", "C4x", "D0", "C5t", "R1x", "C6z", "B1", "T6t", "R2z", "R0t", "D1",
+    "C7z", "T7x", "A2", "C6x", "R3z", "B2", "R1t", "R4z", "D2", "R5t", "R2x", "A3",
+    "R0x", "B3", "R6t", "D3", "R7z", "S3", "R3x", "S0", "R4t", "W0", "R5x", "R2t",
+    "R1z", "R6z", "R7x", "W3", "R3t", "W7", "R4x", "S1", "S2", "R0z", "R5z", "W10",
+    "W5", "W4", "R6x", "R7t", "W2", "W1", "W9", "W8", "W6",
 )
 
 
@@ -46,6 +46,30 @@
 def to_tiles():
     i, j = iota((256, 256), 0), iota((256, 256), 1)
     return (((i >> 3) == (j & 31)) & ((i & 7) == (j >> 5))).astype(F32).astype(BF16)
+
+
+def to_expert_rows():
+    i, j = iota((256, 256), 0), iota((256, 256), 1)
+    place = (((i >> 2) & 3) << 3) | (((i >> 4) & 1) << 2) | (i & 3)
+    return (j == ((place << 3) | (i >> 5))).astype(F32).astype(BF16)
+
+
+def from_expert_rows():
+    j, i = iota((256, 256), 0), iota((256, 256), 1)
+    place = (((i >> 2) & 3) << 3) | (((i >> 4) & 1) << 2) | (i & 3)
+    return (j == ((place << 3) | (i >> 5))).astype(F32).astype(BF16)
+
+
+def to_expert_cols():
+    i, j = iota((256, 256), 0), iota((256, 256), 1)
+    spot = (((i >> 2) & 3) << 6) | ((i >> 5) << 3) | ((i & 3) << 1) | ((i >> 4) & 1)
+    return (j == spot).astype(F32).astype(BF16)
+
+
+def expert_order():
+    i, j = iota((128, 128), 0), iota((128, 128), 1)
+    place = ((i >> 5) << 5) | (((i >> 2) & 3) << 3) | (((i >> 4) & 1) << 2) | (i & 3)
+    return (j == place).astype(F32).astype(BF16)
 
 
 def tile_pair(perm, pieces, put):
@@ -77,7 +101,7 @@
             stat_ref[s, b : b + 1, :] = jnp.sum(part, axis=0, keepdims=True)
 
 
-def routing(routes_ref, gates_ref, index_ref, spot_ref, gate_ref, pick_ref):
+def routing(routes_ref, gates_ref, index_ref, stat_ref, spot_ref, gate_ref, pick_ref):
     head = jnp.concatenate(
         [routes_ref[...].astype(F32), gates_ref[...], jnp.zeros((4, 128), F32)], axis=0
     )
@@ -97,6 +121,7 @@
         index += dot(jnp.where(at, number, 0.0).astype(BF16), one, 0, 0)
         gate += dot(one, jnp.where(at, cols[:, 2 + k : 3 + k], 0.0).astype(BF16), 0, 0)
     index_ref[...] = jnp.clip(index[:8].astype(jnp.int32), 0, 128)
+    stat_ref[2] = index[:8]
     for z in range(4):
         for x in range(4):
             gate_ref[z, x, :, 0, :] = gate[32 * z + 8 * x : 32 * z + 8 * x + 8, :]
@@ -211,7 +236,7 @@
     back_ref, slope_ref, spot_ref, pick_ref, gate_grad, up_grad, down_grad,
     tokens, moe, grad, index_v, index_ref, gate_src, table_ref, stat_ref,
     wg_t, wu_t, wd_t, t_src, t_one, t_two, t_out, c_src, c_one, c_two, c_out, r_one, r_two,
-    g_one, g_two, g_out, q_src, q_one, q_two, s_in, cot_out, cot_in, cot_table,
+    g_one, g_two, g_out, q_src, q_one, q_two, s_in, cot_parts, index_cols, gate_cols,
     x_rows, x_t, d_gate, d_up, hidden, pre_gate, pre_up, cot_rows, back_rows, slope,
     ssem, rsem, lsem, misc, wsem,
 ):
@@ -237,14 +262,13 @@
         load.start()
     greet()
     slope[...] = jnp.zeros((128, 128), F32)
-    unpack_perm, pack_perm = to_rows(), to_tiles()
-    routing(routes_ref, gates_ref, index_v, spot_ref, gate_src, pick_ref)
+    routing(routes_ref, gates_ref, index_v, stat_ref, spot_ref, gate_src, pick_ref)
     index_copy = pltpu.make_async_copy(index_v, index_ref, wsem.at[6])
     index_copy.start()
     need(0, 1)
     statistics(moe, grad, gain_ref, stat_ref)
     need(2)
-    token_table(pack_perm, tokens, table_ref)
+    token_table(to_tiles(), tokens, table_ref)
     index_copy.wait()
     families = {
         "T": (t_src, t_one, t_two, t_out),
@@ -258,7 +282,6 @@
         return tuple(misc.at[i, j] for j in range(3))
 
     stat_hop = Hop("t", 0, stat_ref, s_in, small(0), whole=True)
-    cot_hop = Hop("t", 0, cot_out, cot_in, small(1))
     gate_hops = [
         Hop(d, AXIS[d], a, b, small(2 + i))
         for i, (d, a, b) in enumerate(
@@ -292,30 +315,35 @@
             rows = slice(128 * b, 128 * (b + 1))
             scaled = gain_ref[...] * grad[rows, :].astype(F32)
             saved = moe[rows, :].astype(F32)
-            cot_out[b] = (
+            cot_parts[b] = (
                 cols[:, b : b + 1] * scaled - saved * cols[:, 8 + b : 9 + b]
             ).astype(BF16)
-        begin(cot_hop)
+        index_cols[...] = jnp.concatenate(
+            [s_in[b, 2] for b in range(8)] + [jnp.zeros((64, 128), F32)], axis=0
+        ).T
         gate_hops[0].arrived()
         begin(gate_hops[1])
 
-    def cotangent_table():
-        cot_hop.arrived()
-        for h in range(2):
-            cot_table[h, 0] = jnp.zeros((8, 128), BF16)
-
-            def pieces(g, h=h):
-                return [
-                    cot_in[4 * h + b // 2, 32 * g : 32 * (g + 1), b % 2 * 128 : b % 2 * 128 + 128]
-                    for b in range(8)
-                ]
-
-            def put(g, tiles, h=h):
-                cot_table[h, 1 + 32 * g : 33 + 32 * g] = tiles.reshape(32, 8, 128)
-
-            tile_pair(pack_perm, pieces, put)
-        gate_hops[1].arrived()
-        begin(gate_hops[2])
+    def pack_cotangents(c, dst):
+        rank, half = c // 2, c % 2
+        number = (iota((128, 128), 1) + 1).astype(F32)
+        parts = []
+        for b in range(4 * half, 4 * half + 4):
+            index = index_cols[:, 8 * b + rank : 8 * b + rank + 1]
+            chosen = (index == number).astype(F32).astype(BF16)
+            parts.append(dot(chosen, cot_parts[b]).astype(BF16))
+
+        def pieces(g):
+            return [
+                part[32 * g : 32 * (g + 1), 128 * b : 128 * (b + 1)]
+                for part in parts
+                for b in range(2)
+            ]
+
+        def put(g, tiles):
+            dst[g] = tiles.reshape(4, 8, 8, 128)
+
+        tile_pair(to_tiles(), pieces, put)
 
     def unpack(src, dst, row, half):
         def put(g, b, rows):
@@ -323,7 +351,19 @@
                 row + 32 * g : row + 32 * (g + 1), 1024 * half + 128 * b : 1024 * half + 128 * b + 128
             ] = rows
 
-        row_pair(unpack_perm, lambda g: src[g].reshape(256, 128), put)
+        row_pair(to_expert_rows(), lambda g: src[g].reshape(256, 128), put)
+
+    def unpack_cotangents(src, row, half):
+        perm = to_expert_cols()
+        for pair in range(2):
+            both = jnp.concatenate([src[2 * pair + j].reshape(256, 128) for j in range(2)], axis=1)
+            out = dot(perm, both).astype(BF16)
+            for j in range(2):
+                at = row + 32 * (2 * pair + j) + 16 * half
+                for b in range(16):
+                    cot_rows[at : at + 16, 128 * b : 128 * (b + 1)] = out[
+                        16 * b : 16 * (b + 1), 128 * j : 128 * (j + 1)
+                    ]
 
     def hidden_inputs(r):
         need(3, 4)
@@ -368,20 +408,21 @@
         def put(g, tiles):
             t_src[2 * r + h, g] = tiles.reshape(4, 8, 8, 128)
 
-        tile_pair(pack_perm, pieces, put)
+        tile_pair(from_expert_rows(), pieces, put)
 
     def gate_of(r):
-        gates = jnp.concatenate(
-            [g_out[z, x][:, 0, :] for z in range(4) for x in range(4)], axis=0
-        )
-        return gates[:, r : r + 1]
+        return gate_cols[:, r : r + 1]
 
     def slopes(r):
         if r == 0:
             gate_hops[2].arrived()
+            gates = jnp.concatenate(
+                [g_out[z, x][:, 0, :] for z in range(4) for x in range(4)], axis=0
+            )
+            gate_cols[...] = dot(expert_order(), gates.astype(BF16))
         for h in range(2):
             hops["C", 2 * r + h][2].arrived()
-            unpack(c_out.at[2 * r + h], cot_rows, 128 * r, h)
+            unpack_cotangents(c_out.at[2 * r + h], 128 * r, h)
         gate = gate_of(r)
         rows = slice(128 * r, 128 * (r + 1))
 
@@ -404,7 +445,8 @@
 
     def rest(r):
         half_back(r, 1)
-        if r == 2:
+        if r == 3:
+            slope[...] = dot(expert_order(), slope[...].astype(BF16), 0, 0)
             for z in range(4):
                 for x in range(4):
                     q_src[z, x, :, 0, :] = slope[32 * z + 8 * x : 32 * z + 8 * x + 8, :]
@@ -447,7 +489,11 @@
 
         lax.fori_loop(0, 2, body, 0)
 
-    lasts = (86, 98)
+    early = [step for step in PLAN if step[0] == "T"][:3]
+    for step in early:
+        c = int(step[1])
+        pack(index_ref, c // 2, table_ref, c % 2, t_src.at[c])
+    lasts = (85, 94)
     for i, step in enumerate(PLAN):
         kind = step[0]
         if step == "bar":
@@ -456,8 +502,6 @@
             norm_statistics()
         elif step == "cot":
             cotangents()
-        elif step == "table":
-            cotangent_table()
         elif kind == "A":
             hidden_inputs(int(step[1]))
         elif kind == "B":
@@ -477,10 +521,10 @@
             bufs = families[kind]
             if k:
                 done[-1].arrived()
-            elif kind == "T":
+            elif kind == "T" and step not in early:
                 pack(index_ref, c // 2, table_ref, c % 2, t_src.at[c])
             elif kind == "C":
-                pack(index_ref, c // 2, cot_table, c % 2, c_src.at[c])
+                pack_cotangents(c, c_src.at[c])
             n = "TCR".index(kind) * 8 + c
             hop = Hop(
                 d, AXIS[d], bufs[k].at[c], bufs[k + 1].at[c],
@@ -488,6 +532,9 @@
             )
             begin(hop)
             done.append(hop)
+            if i == 21:
+                gate_hops[1].arrived()
+                begin(gate_hops[2])
             if i in (lasts[0], lasts[1]):
                 slope_hops[lasts.index(i)].arrived()
                 begin(slope_hops[lasts.index(i) + 1])
@@ -499,8 +546,8 @@
 
 
 def finish_kernel(
-    spot_ref, back_ref, slope_ref, pick_ref, gate_grad, up_grad, down_grad,
-    token_ref, gates_ref, gate_out, up_out, down_out, sums, sem,
+    spot_any, back_ref, slope_ref, pick_ref, gate_grad, up_grad, down_grad,
+    token_ref, gates_ref, gate_out, up_out, down_out, spot_ref, sums, sem,
 ):
     copies = [
         pltpu.make_async_copy(a, b.at[0], sem.at[i])
@@ -508,19 +555,22 @@
             ((gate_grad, gate_out), (up_grad, up_out), (down_grad, down_out))
         )
     ]
+    spots = pltpu.make_async_copy(spot_any, spot_ref, sem.at[3])
+    spots.start()
     for copy in copies:
         copy.start()
+    spots.wait()
 
     def body(i, carry):
-        for j in range(8):
-            t = i * 8 + j
+        for j in range(16):
+            t = i * 16 + j
             for h in range(2):
                 one = back_ref[spot_ref[0, t] + 128 * h].astype(F32)
                 two = back_ref[spot_ref[1, t] + 128 * h].astype(F32)
                 sums[h, t] = (one + two).astype(BF16)
         return carry
 
-    lax.fori_loop(0, 16, body, 0)
+    lax.fori_loop(0, 8, body, 0)
     perm = to_rows()
     for h in range(2):
 
@@ -556,7 +606,7 @@
         out_shape=(
             pltpu.VMEM(pieces, BF16),
             pltpu.VMEM(lanes, F32),
-            struct((8, 128), jnp.int32),
+            pltpu.VMEM((8, 128), jnp.int32),
             pltpu.VMEM((128, 128), F32),
             pltpu.VMEM(deep, BF16),
             pltpu.VMEM(deep, BF16),
@@ -572,16 +622,16 @@
             pltpu.SMEM((8, 128), jnp.int32),
             pltpu.VMEM(lanes, F32),
             pltpu.VMEM((2, 129, 8, 128), BF16),
-            pltpu.VMEM((2, 8, 128), F32),
+            pltpu.VMEM((3, 8, 128), F32),
             pltpu.VMEM(flat, BF16),
             pltpu.VMEM(flat, BF16),
             pltpu.VMEM(deep, BF16),
             *[pltpu.VMEM(pieces, BF16)] * 10,
             *[pltpu.VMEM(lanes, F32)] * 6,
-            pltpu.VMEM((8, 2, 8, 128), F32),
+            pltpu.VMEM((8, 3, 8, 128), F32),
             pltpu.VMEM((8, 128, 256), BF16),
-            pltpu.VMEM((8, 128, 256), BF16),
-            pltpu.VMEM((2, 129, 8, 128), BF16),
+            pltpu.VMEM((128, 128), F32),
+            pltpu.VMEM((128, 128), F32),
             pltpu.VMEM((128, 2048), BF16),
             pltpu.VMEM((2048, 512), BF16),
             pltpu.VMEM(inner, BF16),
@@ -615,9 +665,13 @@
             struct((1, *deep)),
             struct((1, *flat)),
         ),
-        in_specs=[SMEM] + [VMEM] * 6,
+        in_specs=[VMEM] * 7,
         out_specs=(VMEM, VMEM, ANY, ANY, ANY),
-        scratch_shapes=[pltpu.VMEM((2, 128, 8, 128), BF16), pltpu.SemaphoreType.DMA((3,))],
+        scratch_shapes=[
+            pltpu.SMEM((8, 128), jnp.int32),
+            pltpu.VMEM((2, 128, 8, 128), BF16),
+            pltpu.SemaphoreType.DMA((4,)),
+        ],
         compiler_params=pltpu.CompilerParams(vmem_limit_bytes=8 << 20),
         name="finish",
     )(spot, back.reshape(1024, 8, 128), slope.reshape(128, 1, 128), pick, gate_grad, up_grad, down_grad)

time: 96.7 us -> 92.5 us (0.957)
  Pallas kernels: 95.1 us -> 91.6 us
    pallas_call x1, Pallas kernels: 89.9 us -> 87 us  [local(): pl.pallas_call(mega_kernel, out_shape=(pltpu.VMEM(pieces, BF16), pltpu.VM...]
where the time goes in v3:
time: 92.5 us; the launch traced here: 92.4 us
  Pallas kernels  91.6 us (99%)
    pallas_call x1, Pallas kernels, local(): pl.pallas_call(mega_kernel, out_shape=(pltpu.VMEM(pieces, BF16), pltpu.VM...  87 us
    pallas_call x1, Pallas kernels, local(): pl.pallas_call(finish_kernel, out_shape=(struct((128, 2048)), struct((2,...  4.57 us

profile of v3, /device:TPU:1, one launch (start us, length us, event | category | flops | bytes accessed | tf_op | source)
XLA Modules:
  0.0 92.4 jit_solution(3091346112366498526)
XLA Ops:
  0.6 87.0 %exchange.1 = (bf16[8,4,4,8,8,128]{5,4,3,2,1,0:T(8,128)(2,1)S(1)}, f32[4,4,8,1,128]{4,3,2,1,0:T(1,128)S(1)}, s32[8,128]{1,0:T(8,128)S(1)}, f32[128,128]{1,0:T(8,...) custom-call(s32[2,128]{1,0:T(2,128)} %bitcast.14, ...), custom_call_target="tpu_custom_call" | custom-call | tf_op jit(solution)/shard_map/exchange/pallas_call | solution.py:604
  87.7 4.6 %finish.1 = (bf16[128,2048]{1,0:T(8,128)(2,1)}, bf16[2,128]{1,0:T(2,128)(2,1)}, bf16[1,2048,768]{2,1,0:T(8,128)(2,1)}, bf16[1,2048,768]{2,1,0:T(8,128)(2,1)}, bf16[1,768,2048]{2,1,0:T(8,128)(2,1)}) custom-call(s32[8,128]{1,0:T(8,128)S(1)} %get-tuple-element.17.spot_any, bf16[1024,8,128]{2,1,0:T(8,128)(2,1)S(1)} %bitcast.9, f32[128,1,128]{2,1,0:T(1,128)S(1)} %bitcast.10, ...), custom_call_target="tpu_custom_call" | custom-call | tf_op jit(solution)/shard_map/finish/pallas_call | solution.py:659

commit v4 on v3

--- a/solution.py
+++ b/solution.py
@@ -16,15 +16,17 @@
 epsilon = 1e-06
 
 PLAN = (
-    "bar", "stat", "T3t", "T2z", "T0t", "T6x", "T1z", "T7z", "T4t", "T5x", "cot", "C0x",
-    "C1t", "C5z", "C2t", "T2x", "T0z", "T1t", "C7t", "M0", "T3x", "C3x", "C4t", "M1",
-    "C0z", "T5z", "C1x", "C2z", "T0x", "C0t", "T1x", "C3z", "C1z", "C6t", "M2", "T2t",
-    "T3z", "T4x", "C5x", "C3t", "C2x", "C4z", "T7t", "C7x", "T5t", "T6z", "A0", "B0",
-    "T4z", "A1", "C4x", "D0", "C5t", "R1x", "C6z", "B1", "T6t", "R2z", "R0t", "D1",
-    "C7z", "T7x", "A2", "C6x", "R3z", "B2", "R1t", "R4z", "D2", "R5t", "R2x", "A3",
-    "R0x", "B3", "R6t", "D3", "R7z", "S3", "R3x", "S0", "R4t", "W0", "R5x", "R2t",
-    "R1z", "R6z", "R7x", "W3", "R3t", "W7", "R4x", "S1", "S2", "R0z", "R5z", "W10",
-    "W5", "W4", "R6x", "R7t", "W2", "W1", "W9", "W8", "W6",
+    "bar", "stat", "T1x", "T0z", "T3t", "T7z", "T6x", "T2z", "T4t", "T5x", "T1t", "cot",
+    "C6z", "C5t", "C4x", "C7z", "C2t", "T4x", "C1t", "T5z", "T7x", "M1", "C4t", "C0x",
+    "C6t", "C5z", "T6z", "C7x", "T4z", "T5t", "M0", "C1x", "C4z", "C0z", "M2", "C5x",
+    "T0x", "T7t", "C6x", "C3z", "T1z", "C2x", "T6t", "C7t", "T2t", "A2", "B2", "D2",
+    "R5z1", "T0t", "T3x", "C1z", "A3", "S2", "C3x", "C0t", "B3", "R6z0", "D3", "R7t0",
+    "R7x1", "R6t1", "T3z", "T2x", "R4z1", "C2z", "R4x0", "A0", "R6t0", "R5x0", "C3t", "B0",
+    "R0z0", "R0t1", "R7t1", "R6x1", "D0", "R1z1", "R1z0", "R4t1", "R6x0", "A1", "R5z0", "R7x0",
+    "R4t0", "R5x1", "B1", "R2x0", "R2t1", "R6z1", "D1", "S1", "R3x0", "R3z1", "R0t0", "W6",
+    "R0x1", "R7z1", "W5", "R7z0", "R1t1", "R4x1", "W1", "R2t0", "S0", "R2z1", "R1x0", "R3t0",
+    "W2", "R3x1", "R4z0", "R5t0", "R0x0", "W3", "R5t1", "R0z1", "R2z0", "R1x1", "R1t0", "R2x1",
+    "S3", "R3z0", "R3t1", "W9", "W7", "W4", "W10", "W0", "W8",
 )
 
 
@@ -157,10 +159,10 @@
 
 def peers(dim, here):
     if dim != "t":
-        return [(here + k) % 4 for k in (1, 3, 2)]
+        return [(here + k) % 4 for k in (2, 1, 3)]
     return [
         (here // 2 + dy) % 4 * 2 + (here % 2 + dc) % 2
-        for dy, dc in ((1, 0), (3, 0), (1, 1), (3, 1), (2, 0), (2, 1), (0, 1))
+        for dy, dc in ((2, 0), (2, 1), (1, 0), (3, 0), (1, 1), (3, 1), (0, 1))
     ]
 
 
@@ -222,6 +224,45 @@
         pltpu.make_async_copy(part, part, self.ssem).wait()
 
 
+class PartHop(Hop):
+    def __init__(self, dim, part, src, dst, sems):
+        core = lax.axis_index("tp") % 2
+        kind = core if part == 0 else 1 - core
+        self.cross = dim == "t" and part == 1
+        self.far = dst.at[:, :, :, 1 - kind]
+        src, dst = src.at[:, :, :, kind], dst.at[:, :, :, kind]
+        super().__init__(dim, AXIS[dim], src, dst, sems)
+
+    def start(self):
+        if self.dim != "t":
+            super().start()
+            return
+        me = coords()
+        mine, core = me["t"] // 2, me["t"] % 2
+        for k in (2, 1, 3, 0) if self.cross else (2, 1, 3):
+            p = (mine + k) % 4
+            place = 2 * p + (1 - core if self.cross else core)
+            pltpu.make_async_remote_copy(
+                cut(self.src, 2, p),
+                cut(self.far if self.cross else self.dst, 2, mine),
+                self.ssem,
+                self.rsem,
+                device_id=(me["z"] * 4 + me["x"], place),
+                device_id_type=MESH,
+            ).start()
+        if not self.cross:
+            pltpu.make_async_copy(cut(self.src, 2, mine), cut(self.dst, 2, mine), self.lsem).start()
+
+    def remote_part(self):
+        return self.dst if self.cross else cut(self.dst, self.axis, slice(0, 3))
+
+    def arrived(self):
+        if self.cross:
+            pltpu.make_async_copy(self.dst, self.dst, self.rsem).wait()
+        else:
+            super().arrived()
+
+
 def pack(index_ref, rank, table_ref, half, dst):
     def body(i, carry):
         for t in range(8):
@@ -235,7 +276,7 @@
     routes_ref, gates_ref, gain_ref, tokens_any, moe_any, grad_any, wg_any, wu_any, wd_any,
     back_ref, slope_ref, spot_ref, pick_ref, gate_grad, up_grad, down_grad,
     tokens, moe, grad, index_v, index_ref, gate_src, table_ref, stat_ref,
-    wg_t, wu_t, wd_t, t_src, t_one, t_two, t_out, c_src, c_one, c_two, c_out, r_one, r_two,
+    wg_t, wu_t, wd_t, t_src, t_one, t_two, t_out, c_src, c_one, c_two, c_out, r_src, r_one, r_two,
     g_one, g_two, g_out, q_src, q_one, q_two, s_in, cot_parts, index_cols, gate_cols,
     x_rows, x_t, d_gate, d_up, hidden, pre_gate, pre_up, cot_rows, back_rows, slope,
     ssem, rsem, lsem, misc, wsem,
@@ -273,7 +314,7 @@
     families = {
         "T": (t_src, t_one, t_two, t_out),
         "C": (c_src, c_one, c_two, c_out),
-        "R": (t_src, r_one, r_two, back_ref),
+        "R": (r_src, r_one, r_two, back_ref),
     }
     hops = {}
     every = []
@@ -398,15 +439,13 @@
 
         lax.fori_loop(0, 2, body, 0)
 
-        hops["T", 2 * r + h][0].left()
-
         def pieces(g):
             return [
                 back_rows[32 * g : 32 * (g + 1), 128 * b : 128 * (b + 1)] for b in range(8)
             ]
 
         def put(g, tiles):
-            t_src[2 * r + h, g] = tiles.reshape(4, 8, 8, 128)
+            r_src[2 * r + h, g] = tiles.reshape(4, 4, 2, 8, 128)
 
         tile_pair(from_expert_rows(), pieces, put)
 
@@ -414,7 +453,7 @@
         return gate_cols[:, r : r + 1]
 
     def slopes(r):
-        if r == 0:
+        if r == 2:
             gate_hops[2].arrived()
             gates = jnp.concatenate(
                 [g_out[z, x][:, 0, :] for z in range(4) for x in range(4)], axis=0
@@ -445,7 +484,7 @@
 
     def rest(r):
         half_back(r, 1)
-        if r == 3:
+        if r == 1:
             slope[...] = dot(expert_order(), slope[...].astype(BF16), 0, 0)
             for z in range(4):
                 for x in range(4):
@@ -493,7 +532,7 @@
     for step in early:
         c = int(step[1])
         pack(index_ref, c // 2, table_ref, c % 2, t_src.at[c])
-    lasts = (85, 94)
+    lasts = (103, 115)
     for i, step in enumerate(PLAN):
         kind = step[0]
         if step == "bar":
@@ -516,7 +555,8 @@
             weight_grad(int(step[1:]))
         else:
             c, d = int(step[1]), step[2]
-            done = hops.setdefault((kind, c), [])
+            part = step[3:]
+            done = hops.setdefault((kind, c, part) if part else (kind, c), [])
             k = len(done)
             bufs = families[kind]
             if k:
@@ -525,21 +565,29 @@
                 pack(index_ref, c // 2, table_ref, c % 2, t_src.at[c])
             elif kind == "C":
                 pack_cotangents(c, c_src.at[c])
-            n = "TCR".index(kind) * 8 + c
-            hop = Hop(
-                d, AXIS[d], bufs[k].at[c], bufs[k + 1].at[c],
-                (ssem.at[n, k], rsem.at[n, k], lsem.at[n, k]),
-            )
+            if part:
+                n = 16 + 2 * c + int(part)
+                hop = PartHop(
+                    d, int(part), bufs[k].at[c], bufs[k + 1].at[c],
+                    (ssem.at[n, k], rsem.at[n, k], lsem.at[n, k]),
+                )
+            else:
+                n = "TC".index(kind) * 8 + c
+                hop = Hop(
+                    d, AXIS[d], bufs[k].at[c], bufs[k + 1].at[c],
+                    (ssem.at[n, k], rsem.at[n, k], lsem.at[n, k]),
+                )
             begin(hop)
             done.append(hop)
-            if i == 21:
+            if i == 22:
                 gate_hops[1].arrived()
                 begin(gate_hops[2])
             if i in (lasts[0], lasts[1]):
                 slope_hops[lasts.index(i)].arrived()
                 begin(slope_hops[lasts.index(i) + 1])
     for c in range(8):
-        hops["R", c][2].arrived()
+        hops["R", c, "0"][2].arrived()
+        hops["R", c, "1"][2].arrived()
     slope_hops[2].arrived()
     for hop in every:
         hop.left()
@@ -547,15 +595,15 @@
 
 def finish_kernel(
     spot_any, back_ref, slope_ref, pick_ref, gate_grad, up_grad, down_grad,
-    token_ref, gates_ref, gate_out, up_out, down_out, spot_ref, sums, sem,
+    token_out, gates_ref, gate_out, up_out, down_out, spot_ref, token_ref, sums, sem,
 ):
-    copies = [
-        pltpu.make_async_copy(a, b.at[0], sem.at[i])
-        for i, (a, b) in enumerate(
-            ((gate_grad, gate_out), (up_grad, up_out), (down_grad, down_out))
-        )
-    ]
-    spots = pltpu.make_async_copy(spot_any, spot_ref, sem.at[3])
+    copies = []
+    for i, (a, b) in enumerate(((gate_grad, gate_out), (up_grad, up_out), (down_grad, down_out))):
+        size = a.shape[0] // 4
+        for j in range(4):
+            part = pl.ds(j * size, size)
+            copies.append(pltpu.make_async_copy(a.at[part], b.at[0, part], sem.at[4 * i + j]))
+    spots = pltpu.make_async_copy(spot_any, spot_ref, sem.at[12])
     spots.start()
     for copy in copies:
         copy.start()
@@ -578,6 +626,8 @@
             token_ref[32 * g : 32 * (g + 1), 1024 * h + 128 * b : 1024 * h + 128 * (b + 1)] = rows
 
         row_pair(perm, lambda g, h=h: sums[h, 32 * g : 32 * (g + 1)].reshape(256, 128), put)
+    copies.append(pltpu.make_async_copy(token_ref, token_out, sem.at[13]))
+    copies[-1].start()
     slope = slope_ref[:, 0, :].astype(BF16)
     pick = pick_ref[...]
     lane = iota((128, 128), 1)
@@ -598,13 +648,14 @@
 
 def local(tokens, routes, gates, w_gate, w_up, w_down, moe_out, norm_gain, out_grad):
     pieces = (8, 4, 4, 8, 8, 128)
+    halves = (8, 4, 4, 4, 2, 8, 128)
     lanes = (4, 4, 8, 1, 128)
     deep, flat = (2048, 768), (768, 2048)
     rows, inner = (512, 2048), (512, 768)
     back, slope, spot, pick, gate_grad, up_grad, down_grad = pl.pallas_call(
         mega_kernel,
         out_shape=(
-            pltpu.VMEM(pieces, BF16),
+            pltpu.VMEM(halves, BF16),
             pltpu.VMEM(lanes, F32),
             pltpu.VMEM((8, 128), jnp.int32),
             pltpu.VMEM((128, 128), F32),
@@ -626,7 +677,8 @@
             pltpu.VMEM(flat, BF16),
             pltpu.VMEM(flat, BF16),
             pltpu.VMEM(deep, BF16),
-            *[pltpu.VMEM(pieces, BF16)] * 10,
+            *[pltpu.VMEM(pieces, BF16)] * 8,
+            *[pltpu.VMEM(halves, BF16)] * 3,
             *[pltpu.VMEM(lanes, F32)] * 6,
             pltpu.VMEM((8, 3, 8, 128), F32),
             pltpu.VMEM((8, 128, 256), BF16),
@@ -642,14 +694,14 @@
             pltpu.VMEM(rows, BF16),
             pltpu.VMEM((128, 1024), BF16),
             pltpu.VMEM((128, 128), F32),
-            pltpu.SemaphoreType.DMA((24, 3)),
-            pltpu.SemaphoreType.DMA((24, 3)),
-            pltpu.SemaphoreType.DMA((24, 3)),
+            pltpu.SemaphoreType.DMA((32, 3)),
+            pltpu.SemaphoreType.DMA((32, 3)),
+            pltpu.SemaphoreType.DMA((32, 3)),
             pltpu.SemaphoreType.DMA((8, 3)),
             pltpu.SemaphoreType.DMA((7,)),
         ],
         compiler_params=pltpu.CompilerParams(
-            collective_id=0, has_side_effects=True, vmem_limit_bytes=46 << 20
+            collective_id=0, has_side_effects=True, vmem_limit_bytes=48 << 20
         ),
         name="exchange",
     )(
@@ -666,11 +718,12 @@
             struct((1, *flat)),
         ),
         in_specs=[VMEM] * 7,
-        out_specs=(VMEM, VMEM, ANY, ANY, ANY),
+        out_specs=(ANY, VMEM, ANY, ANY, ANY),
         scratch_shapes=[
             pltpu.SMEM((8, 128), jnp.int32),
+            pltpu.VMEM((128, 2048), BF16),
             pltpu.VMEM((2, 128, 8, 128), BF16),
-            pltpu.SemaphoreType.DMA((4,)),
+            pltpu.SemaphoreType.DMA((14,)),
         ],
         compiler_params=pltpu.CompilerParams(vmem_limit_bytes=8 << 20),
         name="finish",

time: 92.5 us -> 91 us (0.984)
  Pallas kernels: 91.6 us -> 90.1 us
    pallas_call x1, Pallas kernels: 87 us -> 85.7 us  [local(): pl.pallas_call(mega_kernel, out_shape=(pltpu.VMEM(halves, BF16), pltpu.VM...]
where the time goes in v4:
time: 91 us; the launch traced here: 90.9 us
  Pallas kernels  90.1 us (99%)
    pallas_call x1, Pallas kernels, local(): pl.pallas_call(mega_kernel, out_shape=(pltpu.VMEM(halves, BF16), pltpu.VM...  85.7 us
    pallas_call x1, Pallas kernels, local(): pl.pallas_call(finish_kernel, out_shape=(struct((128, 2048)), struct((2,...  4.4 us

profile of v4, /device:TPU:1, one launch (start us, length us, event | category | flops | bytes accessed | tf_op | source)
XLA Modules:
  0.0 90.9 jit_solution(15500558699018914534)
XLA Ops:
  0.6 85.7 %exchange.1 = (bf16[8,4,4,4,2,8,128]{6,5,4,3,2,1,0:T(8,128)(2,1)S(1)}, f32[4,4,8,1,128]{4,3,2,1,0:T(1,128)S(1)}, s32[8,128]{1,0:T(8,128)S(1)}, f32[128,128]{1,0:...) custom-call(s32[2,128]{1,0:T(2,128)} %bitcast.14, ...), custom_call_target="tpu_custom_call" | custom-call | tf_op jit(solution)/shard_map/exchange/pallas_call | solution.py:655
  86.4 4.4 %finish.1 = (bf16[128,2048]{1,0:T(8,128)(2,1)}, bf16[2,128]{1,0:T(2,128)(2,1)}, bf16[1,2048,768]{2,1,0:T(8,128)(2,1)}, bf16[1,2048,768]{2,1,0:T(8,128)(2,1)}, bf16[1,768,2048]{2,1,0:T(8,128)(2,1)}) custom-call(s32[8,128]{1,0:T(8,128)S(1)} %get-tuple-element.17.spot_any, bf16[1024,8,128]{2,1,0:T(8,128)(2,1)S(1)} %bitcast.9, f32[128,1,128]{2,1,0:T(1,128)S(1)} %bitcast.10, ...), custom_call_target="tpu_custom_call" | custom-call | tf_op jit(solution)/shard_map/finish/pallas_call | solution.py:711

commit v5 on v4

--- a/solution.py
+++ b/solution.py
@@ -273,9 +273,9 @@
 
 
 def mega_kernel(
-    routes_ref, gates_ref, gain_ref, tokens_any, moe_any, grad_any, wg_any, wu_any, wd_any,
+    routes_any, gates_any, gain_any, tokens_any, moe_any, grad_any, wg_any, wu_any, wd_any,
     back_ref, slope_ref, spot_ref, pick_ref, gate_grad, up_grad, down_grad,
-    tokens, moe, grad, index_v, index_ref, gate_src, table_ref, stat_ref,
+    routes_ref, gates_ref, gain_ref, tokens, moe, grad, index_v, index_ref, gate_src, table_ref, stat_ref,
     wg_t, wu_t, wd_t, t_src, t_one, t_two, t_out, c_src, c_one, c_two, c_out, r_src, r_one, r_two,
     g_one, g_two, g_out, q_src, q_one, q_two, s_in, cot_parts, index_cols, gate_cols,
     x_rows, x_t, d_gate, d_up, hidden, pre_gate, pre_up, cot_rows, back_rows, slope,
@@ -288,6 +288,7 @@
             (
                 (moe_any, moe), (grad_any, grad), (tokens_any, tokens),
                 (wg_any, gate_grad), (wu_any, up_grad), (wd_any, down_grad),
+                (routes_any, routes_ref), (gates_any, gates_ref), (gain_any, gain_ref),
             )
         )
     ]
@@ -299,12 +300,13 @@
                 loads[i].wait()
                 loaded.add(i)
 
-    for load in loads:
-        load.start()
     greet()
+    for i in (6, 7, 8, 0, 1, 2, 3, 4, 5):
+        loads[i].start()
     slope[...] = jnp.zeros((128, 128), F32)
+    need(6, 7, 8)
     routing(routes_ref, gates_ref, index_v, stat_ref, spot_ref, gate_src, pick_ref)
-    index_copy = pltpu.make_async_copy(index_v, index_ref, wsem.at[6])
+    index_copy = pltpu.make_async_copy(index_v, index_ref, wsem.at[9])
     index_copy.start()
     need(0, 1)
     statistics(moe, grad, gain_ref, stat_ref)
@@ -663,9 +665,12 @@
             pltpu.VMEM(deep, BF16),
             pltpu.VMEM(flat, BF16),
         ),
-        in_specs=[VMEM] * 3 + [ANY] * 6,
+        in_specs=[ANY] * 9,
         out_specs=(VMEM,) * 7,
         scratch_shapes=[
+            pltpu.VMEM((2, 128), jnp.int32),
+            pltpu.VMEM((2, 128), F32),
+            pltpu.VMEM((1, 256), F32),
             pltpu.VMEM((128, 2048), BF16),
             pltpu.VMEM((1024, 256), BF16),
             pltpu.VMEM((1024, 256), BF16),
@@ -698,7 +703,7 @@
             pltpu.SemaphoreType.DMA((32, 3)),
             pltpu.SemaphoreType.DMA((32, 3)),
             pltpu.SemaphoreType.DMA((8, 3)),
-            pltpu.SemaphoreType.DMA((7,)),
+            pltpu.SemaphoreType.DMA((10,)),
         ],
         compiler_params=pltpu.CompilerParams(
             collective_id=0, has_side_effects=True, vmem_limit_bytes=48 << 20

time: 91 us -> 90.3 us (level)
  no operation moved by 1% of the time
where the time goes in v5:
time: 90.3 us; the launch traced here: 90.2 us
  Pallas kernels  89.4 us (99%)
    pallas_call x1, Pallas kernels, local(): pl.pallas_call(mega_kernel, out_shape=(pltpu.VMEM(halves, BF16), pltpu.VM...  85 us
    pallas_call x1, Pallas kernels, local(): pl.pallas_call(finish_kernel, out_shape=(struct((128, 2048)), struct((2,...  4.4 us

profile of v5, /device:TPU:1, one launch (start us, length us, event | category | flops | bytes accessed | tf_op | source)
XLA Modules:
  0.0 90.2 jit_solution(15349802564842141440)
XLA Ops:
  0.6 85.0 %exchange.1 = (bf16[8,4,4,4,2,8,128]{6,5,4,3,2,1,0:T(8,128)(2,1)S(1)}, f32[4,4,8,1,128]{4,3,2,1,0:T(1,128)S(1)}, s32[8,128]{1,0:T(8,128)S(1)}, f32[128,128]{1,0:...) custom-call(s32[2,128]{1,0:T(2,128)} %bitcast.14, ...), custom_call_target="tpu_custom_call" | custom-call | tf_op jit(solution)/shard_map/exchange/pallas_call | solution.py:657
  85.6 4.4 %finish.1 = (bf16[128,2048]{1,0:T(8,128)(2,1)}, bf16[2,128]{1,0:T(2,128)(2,1)}, bf16[1,2048,768]{2,1,0:T(8,128)(2,1)}, bf16[1,2048,768]{2,1,0:T(8,128)(2,1)}, bf16[1,768,2048]{2,1,0:T(8,128)(2,1)}) custom-call(s32[8,128]{1,0:T(8,128)S(1)} %get-tuple-element.17.spot_any, bf16[1024,8,128]{2,1,0:T(8,128)(2,1)S(1)} %bitcast.9, f32[128,1,128]{2,1,0:T(1,128)S(1)} %bitcast.10, ...), custom_call_target="tpu_custom_call" | custom-call | tf_op jit(solution)/shard_map/finish/pallas_call | solution.py:716

commit v6 on v5

--- a/solution.py
+++ b/solution.py
@@ -597,7 +597,7 @@
 
 def finish_kernel(
     spot_any, back_ref, slope_ref, pick_ref, gate_grad, up_grad, down_grad,
-    token_out, gates_ref, gate_out, up_out, down_out, spot_ref, token_ref, sums, sem,
+    token_out, gates_out, gate_out, up_out, down_out, spot_ref, token_ref, gates_ref, sums, sem,
 ):
     copies = []
     for i, (a, b) in enumerate(((gate_grad, gate_out), (up_grad, up_out), (down_grad, down_out))):
@@ -640,6 +640,8 @@
         mine = jnp.where(lane_f == pick[:, 4 + k : 5 + k], dot(one, slope), 0.0)
         both = jnp.where(lane == k, jnp.sum(mine, axis=1, keepdims=True), both)
     gates_ref[...] = both.T[:2].astype(BF16)
+    copies.append(pltpu.make_async_copy(gates_ref, gates_out, sem.at[14]))
+    copies[-1].start()
     for copy in copies:
         copy.wait()
 
@@ -723,12 +725,13 @@
             struct((1, *flat)),
         ),
         in_specs=[VMEM] * 7,
-        out_specs=(ANY, VMEM, ANY, ANY, ANY),
+        out_specs=(ANY,) * 5,
         scratch_shapes=[
             pltpu.SMEM((8, 128), jnp.int32),
             pltpu.VMEM((128, 2048), BF16),
+            pltpu.VMEM((2, 128), BF16),
             pltpu.VMEM((2, 128, 8, 128), BF16),
-            pltpu.SemaphoreType.DMA((14,)),
+            pltpu.SemaphoreType.DMA((15,)),
         ],
         compiler_params=pltpu.CompilerParams(vmem_limit_bytes=8 << 20),
         name="finish",

time: 90.3 us -> 89.8 us (level)
  no operation moved by 1% of the time
where the time goes in v6:
time: 89.8 us; the launch traced here: 89.7 us
  Pallas kernels  88.9 us (99%)
    pallas_call x1, Pallas kernels, local(): pl.pallas_call(mega_kernel, out_shape=(pltpu.VMEM(halves, BF16), pltpu.VM...  85 us
    pallas_call x1, Pallas kernels, local(): pl.pallas_call(finish_kernel, out_shape=(struct((128, 2048)), struct((2,...  3.9 us

profile of v6, /device:TPU:1, one launch (start us, length us, event | category | flops | bytes accessed | tf_op | source)
XLA Modules:
  0.0 89.7 jit_solution(12271424894911443438)
XLA Ops:
  0.6 85.0 %exchange.1 = (bf16[8,4,4,4,2,8,128]{6,5,4,3,2,1,0:T(8,128)(2,1)S(1)}, f32[4,4,8,1,128]{4,3,2,1,0:T(1,128)S(1)}, s32[8,128]{1,0:T(8,128)S(1)}, f32[128,128]{1,0:...) custom-call(s32[2,128]{1,0:T(2,128)} %bitcast.14, ...), custom_call_target="tpu_custom_call" | custom-call | tf_op jit(solution)/shard_map/exchange/pallas_call | solution.py:659
  85.6 3.9 %finish.1 = (bf16[128,2048]{1,0:T(8,128)(2,1)}, bf16[2,128]{1,0:T(2,128)(2,1)}, bf16[1,2048,768]{2,1,0:T(8,128)(2,1)}, bf16[1,2048,768]{2,1,0:T(8,128)(2,1)}, bf16[1,768,2048]{2,1,0:T(8,128)(2,1)}) custom-call(s32[8,128]{1,0:T(8,128)S(1)} %get-tuple-element.17.spot_any, bf16[1024,8,128]{2,1,0:T(8,128)(2,1)S(1)} %bitcast.9, f32[128,1,128]{2,1,0:T(1,128)S(1)} %bitcast.10, ...), custom_call_target="tpu_custom_call" | custom-call | tf_op jit(solution)/shard_map/finish/pallas_call | solution.py:718
